TPU v7x, 256 devices: a whole 4x4x8 slice. The times are simulated.
256 devices in a mesh: sp: 32 (over z, x), tp: 4 (over y), dp: 2 (over core).
Axes of the slice: x: 4, y: 4, z: 8, core: 2. Of those that a mesh axis runs over, the one named last changes fastest.
Arguments:
- latent: bfloat16 [2, 6144, 2048], P('dp', 'sp'), may hold values from -6 to 6
- cond: bfloat16 [2, 2048], P('dp', 'sp'), may hold values from -6 to 6
- context: bfloat16 [2, 256, 2048], P('dp', 'sp'), may hold values from -6 to 6
- ctx_cond: bfloat16 [2048], P('sp'), may hold values from -6 to 6
- w_mod: bfloat16 [2048, 6144], P('sp', 'tp'), may hold values from -0.125 to 0.125
- norm_gain: bfloat16 [2048], replicated, may hold values from 0.099609375 to 1.8984375
- w_query: bfloat16 [2048, 1024], P(None, 'tp'), may hold values from -0.125 to 0.125
- w_key: bfloat16 [2048, 1024], P(None, 'tp'), may hold values from -0.125 to 0.125
- w_value: bfloat16 [2048, 1024], P(None, 'tp'), may hold values from -0.125 to 0.125
- w_outgate: bfloat16 [2048, 1024], P(None, 'tp'), may hold values from -0.125 to 0.125
- w_decay: bfloat16 [2048, 2, 8], P(None, None, 'tp'), may hold values from -0.125 to 0.125
- w_beta: bfloat16 [2048, 2, 8], P(None, None, 'tp'), may hold values from -0.125 to 0.125
- decay_rate: float32 [2, 8], P(None, 'tp'), may hold values from 8.138021e-06 to 0.0333333333
- decay_bias: float32 [2, 8], P(None, 'tp'), may hold values from -3 to 3
- extra_decay: float32 [2, 2, 8, 6144], P('dp', None, 'tp', 'sp'), may hold values from -0.7000977 to -1.6276042e-05
- out_gain: bfloat16 [128], replicated, may hold values from 0.099609375 to 1.8984375
- w_out: bfloat16 [1024, 2048], replicated, may hold values from -0.1875 to 0.1875
Outputs:
- mixed_out: bfloat16 [2, 6144, 2048], P('dp', ('sp', 'tp'))
All inputs are finite; a program needn't handle non-finite values.
Results may differ from a plain program's by a relative error of at most 0.0067.
Values may be sent and summed in bfloat16 or wider, within the bound.
No kernel may reach another device: no remote copies, remote signals or barrier semaphores. Data moves between devices by JAX's collectives and lax.ppermute only.
A program may use at most 128 MiB of HBM per device.

v0:
```python
import functools

import jax
import jax.numpy as jnp
from jax import lax
from jax.experimental import pallas as pl
from jax.experimental.pallas import tpu as pltpu
from jax.sharding import Mesh
from jax.sharding import PartitionSpec as P

D = 2048
HEAD = 128
LANES = 128
NORM_EPS = 1e-06
BETA_SCALE = 30.0

SPAN = 192
CTX_OWN = 8
ROWS = 208
CHUNK = 256
CHUNKS = 3
ROW_OF_X = 4 * SPAN

K_AT, V_AT, Q_AT, G_AT, S_AT, X_ROWS = 0, 208, 416, 608, 704, 720
C_AT, D_AT, Z_ROWS = 128, 160, 192

F32 = jnp.float32
BF16 = jnp.bfloat16


def dot(a, b, dims=((1,), (0,))):
    return lax.dot_general(a, b, (dims, ((), ())), preferred_element_type=F32)


def silu(v):
    return v / (1.0 + jnp.exp(-v))


def rounded(v):
    return v.astype(BF16).astype(F32)


def split_in_two(v):
    high = v.astype(BF16)
    return high.astype(F32), v - high.astype(F32)


def iota(shape, dim):
    return lax.broadcasted_iota(jnp.int32, shape, dim)


def partial_modulation(cond, ctx_cond, w_mod, out, rows):
    first = iota((8, cond.shape[1]), 0) == 0
    values = jnp.where(first, cond[...].astype(F32), ctx_cond[...].astype(F32))
    product = dot(silu(values).astype(BF16), w_mod[...])
    for r in range(2):
        for c in range(12):
            rows[r * 12 + c : r * 12 + c + 1, :] = product[r : r + 1, c * LANES : (c + 1) * LANES]
    value = rows[...].astype(BF16)
    for k in range(out.shape[0]):
        out[k] = value


def sum_and_spread(parts, out):
    total = parts[0].astype(F32)
    for k in range(1, parts.shape[0]):
        total = total + parts[k].astype(F32)
    value = total.astype(BF16)
    for k in range(out.shape[0]):
        out[k] = value


def modulated(values, gain, mods, which):
    scale = lax.rsqrt(jnp.mean(values * values, axis=-1, keepdims=True) + NORM_EPS)

    def row(block):
        at = (block // 12) * 24 + which * 12 + block % 12
        return mods[at : at + 1, :]

    out = []
    for j in range(D // LANES):
        cols = slice(j * LANES, (j + 1) * LANES)
        factor = gain[:, cols].astype(F32) * (1.0 + row(16 + j))
        out.append((values[:, cols] * scale * factor + row(j)).astype(BF16))
    return out


def project(
    parts, latent, context, gain, w_query, w_key, w_value, w_gate, w_small, rate, bias, extra,
    out, gate_out, mods, rows_in,
):
    for y in range(4):
        total = parts[y].astype(F32)
        for x in range(1, 4):
            total = total + parts[4 * x + y].astype(F32)
        mods[24 * y : 24 * y + 24, :] = total
    for j in range(16):
        block = 32 + j
        at = (block // 12) * 24 + block % 12
        gate_out[j : j + 1, :] = mods[at : at + 1, :]
    for g in range(0, SPAN, 64):
        for j, tile in enumerate(modulated(latent[g : g + 64, :].astype(F32), gain, mods, 0)):
            rows_in[g : g + 64, j * LANES : (j + 1) * LANES] = tile
    ctx_values = jnp.concatenate(
        [context[...].astype(F32), jnp.zeros((ROWS - SPAN - CTX_OWN, D), F32)], axis=0
    )
    for j, tile in enumerate(modulated(ctx_values, gain, mods, 1)):
        rows_in[SPAN:ROWS, j * LANES : (j + 1) * LANES] = tile
    inputs = rows_in[...]

    def heads(values):
        return [values[:, h * HEAD : (h + 1) * HEAD] for h in range(2)]

    small = rounded(dot(w_small[...], inputs, ((1,), (1,))))
    decay_raw, beta_raw = small[:4], small[4:]
    pre = decay_raw + bias[...]
    soft = jnp.maximum(pre, 0.0) + jnp.log1p(jnp.exp(-jnp.abs(pre)))
    added = jnp.concatenate([extra[...], jnp.zeros((4, ROWS - SPAN), F32)], axis=1)
    log_decay = -rate[...] * soft + added
    beta = BETA_SCALE * rate[...] / (1.0 + jnp.exp(-beta_raw))
    pad = jnp.zeros((4, 256 - ROWS), F32)
    g_high, g_low = split_in_two(jnp.concatenate([log_decay, pad], axis=1))
    b_high, b_low = split_in_two(jnp.concatenate([beta, pad], axis=1))

    def unit(v):
        return v * lax.rsqrt(jnp.sum(v * v, axis=-1, keepdims=True) + NORM_EPS)

    keys = heads(silu(rounded(dot(inputs, w_key[...]))))
    values = heads(silu(rounded(dot(inputs, w_value[...]))))
    queries = heads(silu(rounded(dot(inputs[:SPAN], w_query[...]))))
    gates = heads(silu(rounded(dot(inputs[:SPAN], w_gate[...]))))
    low_lanes = iota((24, LANES), 1) < 64
    for h in range(2):
        key = unit(keys[h]).astype(BF16)
        value = values[h].astype(BF16)
        query = (unit(queries[h]) * HEAD**-0.5).astype(BF16)
        for d in range(2):
            peer = 2 * h + d
            out[peer, K_AT:V_AT, :] = key
            out[peer, V_AT:Q_AT, :] = value
            out[peer, Q_AT:G_AT, :] = query
            packed = []
            for y in range(4):
                one = gates[h][48 * y : 48 * y + 24]
                two = gates[h][48 * y + 24 : 48 * y + 48]
                if d == 0:
                    packed.append(jnp.where(low_lanes, one, pltpu.roll(two, 64, 1)))
                else:
                    packed.append(jnp.where(low_lanes, pltpu.roll(one, 64, 1), two))
            out[peer, G_AT:S_AT, :] = jnp.concatenate(packed, axis=0).astype(BF16)
            at = 2 * d + h
            four = jnp.concatenate(
                [g_high[at : at + 1], g_low[at : at + 1], b_high[at : at + 1], b_low[at : at + 1],
                 jnp.zeros((4, 256), F32)],
                axis=0,
            )
            out[peer, S_AT:X_ROWS, :] = jnp.concatenate(
                [four[:, :LANES], four[:, LANES:]], axis=0
            ).astype(BF16)


def unit_inverses(lows):
    results = [None] * len(lows)
    largest = max(low.shape[0] for low in lows)
    width = 1
    while width < largest:
        inner = [None] * len(lows)
        for n, low in enumerate(lows):
            size = low.shape[0]
            if width >= size:
                continue
            i, j = iota((size, size), 0), iota((size, size), 1)
            coupled = (i // (2 * width) == j // (2 * width)) & (i // width != j // width)
            coupling = jnp.where(coupled, low, 0.0)
            if width == 1:
                results[n] = jnp.where(i == j, 1.0, 0.0) - coupling
            else:
                inner[n] = (dot(coupling.astype(BF16), results[n].astype(BF16))).astype(BF16)
        if width > 1:
            for n, low in enumerate(lows):
                if inner[n] is not None:
                    results[n] = results[n] - dot(results[n].astype(BF16), inner[n])
        width *= 2
    return results


def token_maps(got, out, reads, offsets, maps, queries):
    backward = lax.rem(lax.axis_index("x"), 2)
    sign = 1 - 2 * backward
    size = CHUNK
    ahead = sign * (iota((size, size), 0) - iota((size, size), 1))
    upto = jnp.where(ahead >= 0, 1.0, 0.0).astype(BF16)
    same = jnp.where(ahead == 0, 1.0, 0.0).astype(BF16)
    low_lanes = iota((8, LANES), 1) < 64

    small = [got[p, S_AT:X_ROWS, :].astype(F32) for p in range(4)]
    first = [s[:8] for s in small]
    second = [s[8:] for s in small]
    turn = lambda v: pltpu.roll(v, 64, 1)
    blocks = [
        first[0],
        jnp.where(low_lanes, second[0], turn(first[1])),
        jnp.where(low_lanes, turn(first[1]), turn(second[1])),
        first[2],
        jnp.where(low_lanes, second[2], turn(first[3])),
        jnp.where(low_lanes, turn(first[3]), turn(second[3])),
    ]
    ctx_lane = iota((8, LANES), 1)
    ctx_small = jnp.zeros((8, LANES), F32)
    for p in range(4):
        here = (ctx_lane >= 8 * p) & (ctx_lane < 8 * p + 8)
        ctx_small = jnp.where(here, pltpu.roll(second[p], (64 + 8 * p) % 128, 1), ctx_small)

    def latent_rows(at, m):
        pieces = {
            0: ((0, 0, 192), (1, 0, 64)),
            1: ((1, 64, 192), (2, 0, 128)),
            2: ((2, 128, 192), (3, 0, 192)),
        }[m]
        return jnp.concatenate([got[p, at + a : at + b, :] for p, a, b in pieces], axis=0)

    def ctx_rows(at):
        return jnp.concatenate(
            [got[p, at + SPAN : at + ROWS, :].astype(F32)[:CTX_OWN] for p in range(4)], axis=0
        ).astype(BF16)

    sets = []
    for m in range(CHUNKS):
        rows = jnp.concatenate([blocks[2 * m], blocks[2 * m + 1]], axis=1).astype(BF16)
        sets.append((latent_rows(K_AT, m), latent_rows(V_AT, m), rows, size, size))
    sets.append((ctx_rows(K_AT), ctx_rows(V_AT), ctx_small.astype(BF16), 32, LANES))

    decays, lows, rights, kept, totals = [], [], [], [], []
    for key, value, rows, n, lanes in sets:
        sums = dot(upto[:n, :lanes], rows, ((1,), (1,)))
        rates = dot(same[:n, :lanes], rows, ((1,), (1,)))
        down = sums[:, 0:1] + sums[:, 1:2]
        beta = rates[:, 2:3] + rates[:, 3:4]
        across = dot(rows, upto[:lanes, :lanes], ((1,), (1,)))
        along = (across[0:1] + across[1:2])[:, :n]
        reach = ahead[:n, :n]
        weights = jnp.where(reach >= 0, jnp.exp(jnp.where(reach >= 0, down - along, 0.0)), 0.0)
        total = jnp.where(backward == 0, down[n - 1 : n], down[0:1])
        key32 = key.astype(F32)
        decayed = jnp.exp(down)
        lows.append(jnp.where(reach > 0, dot(key, key, ((1,), (1,))) * weights * beta, 0.0))
        rights.append(
            jnp.concatenate(
                [(value.astype(F32) * beta).astype(BF16), (key32 * (beta * decayed)).astype(BF16)],
                axis=1,
            )
        )
        kept.append((key32 * jnp.exp(total - down)).astype(BF16))
        totals.append(jnp.exp(total))
        decays.append((decayed, weights))
    inverses = unit_inverses(lows)
    factors = [dot(t.astype(BF16), r).astype(BF16) for t, r in zip(inverses, rights)]

    unit = jnp.where(iota((HEAD, HEAD), 0) == iota((HEAD, HEAD), 1), 1.0, 0.0)
    for m in range(CHUNKS):
        both = dot(kept[m], factors[m], ((0,), (0,)))
        maps[m] = jnp.concatenate([both[:, :HEAD], totals[m] * unit - both[:, HEAD:]], axis=1)
    for m in range(CHUNKS):
        query = latent_rows(Q_AT, m)
        decayed, weights = decays[m]
        pairs = (dot(query, sets[m][0], ((1,), (1,))) * weights).astype(BF16)
        local = dot(pairs, factors[m])
        queries[m] = jnp.concatenate(
            [local[:, :HEAD], query.astype(F32) * decayed - local[:, HEAD:]], axis=1
        )
    so_far = None
    for step in range(CHUNKS):
        m = jnp.where(backward == 0, step, CHUNKS - 1 - step)
        here = queries[m]
        rows = pl.ds(pl.multiple_of(m * CHUNK, CHUNK), CHUNK)
        if step == 0:
            reads[rows, :] = here[:, HEAD:].astype(BF16)
            offsets[rows, :] = here[:, :HEAD]
            so_far = maps[m]
        else:
            moved = dot(here[:, HEAD:].astype(BF16), so_far.astype(BF16))
            reads[rows, :] = moved[:, HEAD:].astype(BF16)
            offsets[rows, :] = here[:, :HEAD] + moved[:, :HEAD]
            mine = maps[m]
            nxt = dot(mine[:, HEAD:].astype(BF16), so_far.astype(BF16))
            so_far = jnp.concatenate([nxt[:, :HEAD] + mine[:, :HEAD], nxt[:, HEAD:]], axis=1)
    whole = so_far.astype(BF16)
    high, low = split_in_two(totals[CHUNKS])
    left = iota((32, LANES), 1) < 64
    tail = jnp.concatenate(
        [kept[CHUNKS], jnp.where(left, high, low).astype(BF16)], axis=1
    )
    for k in range(out.shape[0]):
        out[k, :C_AT, :] = whole
        out[k, C_AT:D_AT, :] = factors[CHUNKS]
        out[k, D_AT:, :] = tail


def read_states(got, reads, offsets, sent, out):
    backward = lax.rem(lax.axis_index("x"), 2)
    place = lax.axis_index("z")
    count = got.shape[0]
    before = jnp.where(backward == 0, place, count - 1 - place)
    ctx_state = jnp.zeros((HEAD, HEAD), F32)
    unit = jnp.where(iota((HEAD, HEAD), 0) == iota((HEAD, HEAD), 1), 1.0, 0.0)
    chain = jnp.concatenate([jnp.zeros((HEAD, HEAD), F32), unit], axis=1)
    for step in range(count):
        k = jnp.where(backward == 0, step, count - 1 - step)
        factor = got[k, C_AT:D_AT, :]
        tail = got[k, D_AT:, :]
        both = tail[0:1, HEAD:].astype(F32)
        kept_share = both[:, 0:1] + both[:, 64:65]
        fresh = factor[:, :HEAD].astype(F32)
        if step > 0:
            fresh = fresh - dot(factor[:, HEAD:], ctx_state.astype(BF16))
        ctx_state = ctx_state * kept_share + dot(tail[:, :HEAD], fresh.astype(BF16), ((0,), (0,)))
        if step < count - 1:
            mine = got[k, :C_AT, :]
            nxt = dot(mine[:, HEAD:], chain.astype(BF16))
            nxt = jnp.concatenate([nxt[:, :HEAD] + mine[:, :HEAD].astype(F32), nxt[:, HEAD:]], axis=1)
            chain = jnp.where(step < before, nxt, chain)
    state = dot(chain[:, HEAD:].astype(BF16), ctx_state.astype(BF16)) + chain[:, :HEAD]
    state = state.astype(BF16)
    for x in range(4):
        rows = slice(SPAN * x, SPAN * x + SPAN)
        o = dot(reads[rows, :], state) + offsets[rows, :]
        gates = sent[x, G_AT:S_AT, :].astype(F32)
        for y in range(4):
            out[4 * x + y] = jnp.concatenate(
                [o[48 * y : 48 * y + 48], gates[24 * y : 24 * y + 24]], axis=0
            ).astype(BF16)


def mix(got, out_gain, gate, w_out, latent, out):
    low_lanes = iota((24, LANES), 1) < 64
    gain = out_gain[...].astype(F32)
    tiles = []
    for y in range(4):
        for h in range(2):
            one = got[8 * h + y].astype(F32)
            two = got[8 * h + 4 + y].astype(F32)
            o = one[:48] + two[:48]
            one, two = one[48:], two[48:]
            gates = jnp.concatenate(
                [
                    jnp.where(low_lanes, one, pltpu.roll(two, 64, 1)),
                    jnp.where(low_lanes, pltpu.roll(one, 64, 1), two),
                ],
                axis=0,
            )
            normed = o * lax.rsqrt(jnp.mean(o * o, axis=-1, keepdims=True) + NORM_EPS)
            tiles.append((normed * gain * gates).astype(BF16))
    gated = jnp.concatenate(tiles, axis=1)
    start = pl.multiple_of(lax.axis_index("tp") * 48, 16)
    own = latent[pl.ds(start, 48), :].astype(F32)
    for n in range(0, D, 512):
        mixed = dot(gated, w_out[:, n : n + 512])
        for c in range(0, 512, LANES):
            j = (n + c) // LANES
            cols = slice(n + c, n + c + LANES)
            out[:, cols] = (own[:, cols] + gate[j : j + 1, :] * mixed[:, c : c + LANES]).astype(BF16)


VM = pl.BlockSpec(memory_space=pltpu.VMEM)


def call(body, name, n_in, outs, scratch=(), mib=16):
    many = isinstance(outs, (list, tuple))
    return pl.pallas_call(
        body,
        out_shape=outs,
        in_specs=[VM] * n_in,
        out_specs=[VM] * len(outs) if many else VM,
        scratch_shapes=list(scratch),
        compiler_params=pltpu.CompilerParams(vmem_limit_bytes=mib << 20),
        name=name,
    )


def shape(dims, dtype=BF16):
    return jax.ShapeDtypeStruct(dims, dtype)


def swap(array, axes):
    return lax.all_to_all(array, axes, 0, 0, tiled=True)


def on_device(
    latent, cond, context, ctx_cond, w_mod, norm_gain, w_query, w_key, w_value, w_outgate,
    w_decay, w_beta, decay_rate, decay_bias, extra_decay, out_gain, w_out,
):
    small = jnp.concatenate([w_decay.reshape(D, 4).T, w_beta.reshape(D, 4).T], axis=0)
    partial = call(
        partial_modulation, "partial_modulation", 3, shape((8, 24, LANES)),
        [pltpu.VMEM((24, LANES), F32)],
    )(cond, ctx_cond[None, :], w_mod)
    summed = call(sum_and_spread, "sum_and_spread", 1, shape((16, 24, LANES)))(swap(partial, "z"))
    parts = swap(summed, ("x", "tp"))
    sent, gate = call(
        project, "project", 12, [shape((4, X_ROWS, LANES)), shape((16, LANES), F32)],
        [pltpu.VMEM((96, LANES), F32), pltpu.VMEM((ROWS, D), BF16)], 24,
    )(
        parts, latent[0], context[0], norm_gain[None, :], w_query, w_key, w_value, w_outgate, small,
        decay_rate.reshape(4, 1), decay_bias.reshape(4, 1), extra_decay.reshape(4, SPAN),
    )
    held = swap(sent, "x")
    maps, reads, offsets = call(
        token_maps, "token_maps", 1,
        [shape((8, Z_ROWS, 256)), shape((ROW_OF_X, HEAD)), shape((ROW_OF_X, HEAD), F32)],
        [pltpu.VMEM((CHUNKS, HEAD, 256), F32), pltpu.VMEM((CHUNKS, CHUNK, 256), F32)],
    )(held)
    reached = swap(maps, "z")
    outs = call(read_states, "read_states", 4, shape((16, 72, LANES)))(
        reached, reads, offsets, held
    )
    own = swap(outs, ("x", "tp"))
    mixed = call(mix, "mix", 5, shape((48, D)))(own, out_gain[None, :], gate, w_out, latent[0])
    return mixed[None]


def solution(mesh):
    torus = Mesh(
        mesh.devices.reshape(8, 4, mesh.shape["tp"], mesh.shape["dp"]), ("z", "x", "tp", "dp")
    )
    sp = ("z", "x")
    return jax.shard_map(
        on_device,
        mesh=torus,
        in_specs=(
            P("dp", sp, None),
            P("dp", sp),
            P("dp", sp, None),
            P(sp),
            P(sp, "tp"),
            P(),
            P(None, "tp"),
            P(None, "tp"),
            P(None, "tp"),
            P(None, "tp"),
            P(None, None, "tp"),
            P(None, None, "tp"),
            P(None, "tp"),
            P(None, "tp"),
            P("dp", None, "tp", sp),
            P(),
            P(),
        ),
        out_specs=P("dp", ("z", "x", "tp"), None),
        check_vma=False,
    )
```

profile of v0, /device:TPU:2, one launch (start us, length us, event | category | flops | bytes accessed | tf_op | source)
XLA Modules:
  0.0 96.5 jit_solution(324100817761563702)
XLA Ops:
  0.0 0.9 copy-done.6
  0.9 0.7 copy-done.8
  1.6 0.7 copy-done.9
  2.2 0.8 partial_modulation.1
  3.0 8.5 %all-to-all-start = ((bf16[8,24,128]{2,1,0:T(8,128)(2,1)}), bf16[8,24,128]{2,1,0:T(8,128)(2,1)S(1)}, u32[]{:S(2)}, u32[]{:S(2)}) async-start(bf16[8,24,128]{2,1,0:T(8,128)(2,1)} %partial_modulation.1), calls=%async_computation | async-start | bytes 98304 | tf_op jit(solution)/shard_map/all_to_all | solution.py:385
  11.5 0.7 reshape.15
  12.2 0.7 reshape.16
  13.0 6.7 %all-to-all-done.parts = bf16[8,24,128]{2,1,0:T(8,128)(2,1)S(1)} async-done(((bf16[8,24,128]{2,1,0:T(8,128)(2,1)}), bf16[8,24,128]{2,1,0:T(8,128)(2,1)S(1)}, u32[]{:S(2)}, u32[]{:S(2)}) %all-to-all-start) | async-done | bytes 49184 | tf_op jit(solution)/shard_map/all_to_all | solution.py:385
  19.7 0.7 sum_and_spread.1
  20.4 7.5 %all-to-all-start.1 = ((bf16[16,24,128]{2,1,0:T(8,128)(2,1)}), bf16[16,24,128]{2,1,0:T(8,128)(2,1)S(1)}, u32[]{:S(2)}, u32[]{:S(2)}) async-start(bf16[16,24,128]{2,1,0:T(8,128)(2,1)} %sum_and_spread.1), calls=%async_computation.1 | async-start | bytes 196608 | tf_op jit(solution)/shard_map/all_to_all | solution.py:385
  27.9 0.8 reshape.20.rate
  28.6 0.8 reshape.21.bias
  29.4 0.7 reshape.19.extra
  30.1 0.7 broadcast_in_dim.13.gain
  30.8 3.4 %all-to-all-done.1.parts = bf16[16,24,128]{2,1,0:T(8,128)(2,1)S(1)} async-done(((bf16[16,24,128]{2,1,0:T(8,128)(2,1)}), bf16[16,24,128]{2,1,0:T(8,128)(2,1)S(1)}, u32[]{:S(2)}, u32[]{:S(2)}) %all-to-all-start.1) | async-done | bytes 98336 | tf_op jit(solution)/shard_map/all_to_all | solution.py:385
  34.2 1.1 %copy-done.1 = bf16[1,192,2048]{2,1,0:T(8,128)(2,1)S(1)} copy-done((bf16[1,192,2048]{2,1,0:T(8,128)(2,1)S(1)}, bf16[1,192,2048]{2,1,0:T(8,128)(2,1)}, u32[]{:S(2)}) %copy-start.1) | copy-done | bytes 786456
  35.3 1.2 %copy-done.2 = bf16[2048,256]{1,0:T(8,128)(2,1)S(1)} copy-done((bf16[2048,256]{1,0:T(8,128)(2,1)S(1)}, bf16[2048,256]{1,0:T(8,128)(2,1)}, u32[]{:S(2)}) %copy-start.2) | copy-done | bytes 1048600
  36.5 1.2 %copy-done.3 = bf16[2048,256]{1,0:T(8,128)(2,1)S(1)} copy-done((bf16[2048,256]{1,0:T(8,128)(2,1)S(1)}, bf16[2048,256]{1,0:T(8,128)(2,1)}, u32[]{:S(2)}) %copy-start.3) | copy-done | bytes 1048600
  37.7 1.2 %copy-done.4 = bf16[2048,256]{1,0:T(8,128)(2,1)S(1)} copy-done((bf16[2048,256]{1,0:T(8,128)(2,1)S(1)}, bf16[2048,256]{1,0:T(8,128)(2,1)}, u32[]{:S(2)}) %copy-start.4) | copy-done | bytes 1048600
  39.0 1.2 %copy-done.5 = bf16[2048,256]{1,0:T(8,128)(2,1)S(1)} copy-done((bf16[2048,256]{1,0:T(8,128)(2,1)S(1)}, bf16[2048,256]{1,0:T(8,128)(2,1)}, u32[]{:S(2)}) %copy-start.5) | copy-done | bytes 1048600
  40.2 0.8 copy-done.7
  40.9 1.8 %project.1 = (bf16[4,720,128]{2,1,0:T(8,128)(2,1)S(1)}, f32[16,128]{1,0:T(8,128)S(1)}) custom-call(bf16[16,24,128]{2,1,0:T(8,128)(2,1)S(1)} %all-to-all-done.1.parts, bf16[192,2048]{1,0:T(8,128)(2,1)S(1)} %bitcast.11, bf16[8,2048]{1,0:T(8,128)(2,1)S(1)} %bitcast.13, bf16[1,2048]{1,0:T(2,128)(2,1)S(1)} %broadcast_in_dim.13.gain, ...), custom_call_target="tpu_custom_call" | custom-call | tf_op jit(solution)/shard_map/project/pallas_call | solution.py:399
  42.7 0.0 copy-start
  42.8 0.0 copy-start.10
  42.8 11.9 %all_to_all.25.got.sent = bf16[4,720,128]{2,1,0:T(8,128)(2,1)S(1)} all-to-all(bf16[4,720,128]{2,1,0:T(8,128)(2,1)S(1)} %get-tuple-element.10), channel_id=1, replica_groups=mesh['z'=8,'x'=4,'tp'=4,'dp'=2] {'x'}, dimensions={0} | all-to-all | bytes 1474560 | tf_op jit(solution)/shard_map/all_to_all | solution.py:385
  54.7 4.4 %token_maps.1 = (bf16[8,192,256]{2,1,0:T(8,128)(2,1)S(1)}, bf16[768,128]{1,0:T(8,128)(2,1)S(1)}, f32[768,128]{1,0:T(8,128)S(1)}) custom-call(bf16[4,720,128]{2,1,0:T(8,128)(2,1)S(1)} %all_to_all.25.got.sent), custom_call_target="tpu_custom_call" | custom-call | tf_op jit(solution)/shard_map/token_maps/pallas_call | solution.py:407
  59.2 21.8 %all_to_all.26.got = bf16[8,192,256]{2,1,0:T(8,128)(2,1)S(1)} all-to-all(bf16[8,192,256]{2,1,0:T(8,128)(2,1)S(1)} %get-tuple-element.11), channel_id=1, replica_groups=mesh['z'=8,'x'=4,'tp'=4,'dp'=2] {'z'}, dimensions={0} | all-to-all | bytes 1572864 | tf_op jit(solution)/shard_map/all_to_all | solution.py:385
  81.0 2.3 %read_states.1 = bf16[16,72,128]{2,1,0:T(8,128)(2,1)S(1)} custom-call(bf16[8,192,256]{2,1,0:T(8,128)(2,1)S(1)} %all_to_all.26.got, bf16[768,128]{1,0:T(8,128)(2,1)S(1)} %get-tuple-element.12.reads, f32[768,128]{1,0:T(8,128)S(1)} %get-tuple-element.13.offsets, bf16[4,720,128]{2,1,0:T(8,128)(2,1)S(1)} %all_to_all.25.got.sent), custom_call_target="tpu_custom_call" | custom-call | tf_op jit(solution)/shard_map/read_states/pallas_call | solution.py:413
  83.3 11.6 %all_to_all.27.got = bf16[16,72,128]{2,1,0:T(8,128)(2,1)S(1)} all-to-all(bf16[16,72,128]{2,1,0:T(8,128)(2,1)S(1)} %read_states.1), channel_id=1, replica_groups=mesh['z'=8,'x'=4,'tp'=4,'dp'=2] {'x','tp'}, dimensions={0} | all-to-all | bytes 589824 | tf_op jit(solution)/shard_map/all_to_all | solution.py:385
  94.9 0.0 copy-done
  94.9 0.0 copy-done.10
  94.9 1.6 %mix.1 = bf16[48,2048]{1,0:T(8,128)(2,1)} custom-call(bf16[16,72,128]{2,1,0:T(8,128)(2,1)S(1)} %all_to_all.27.got, bf16[1,128]{1,0:T(2,128)(2,1)S(1)} %bitcast.15, f32[16,128]{1,0:T(8,128)S(1)} %get-tuple-element.14.gate, bf16[1024,2048]{1,0:T(8,128)(2,1)S(1)} %copy-done, bf16[192,2048]{1,0:T(8,128)(2,1)S(1)} %bitcast.12), custom_call_target="tpu_custom_call" | custom-call | tf_op jit(solution)/shard_map/mix/pallas_call | solution.py:417
  (10 shorter events, 0.0 us)
Async XLA Ops:
  0.0 0.9 copy-start.6
  0.9 0.7 copy-start.8
  1.6 0.7 copy-start.9
  3.0 16.7 %all-to-all-start = ((bf16[8,24,128]{2,1,0:T(8,128)(2,1)}), bf16[8,24,128]{2,1,0:T(8,128)(2,1)S(1)}, u32[]{:S(2)}, u32[]{:S(2)}) async-start(bf16[8,24,128]{2,1,0:T(8,128)(2,1)} %partial_modulation.1), calls=%async_computation | async-start | bytes 98304 | tf_op jit(solution)/shard_map/all_to_all | solution.py:385
  20.4 13.8 %all-to-all-start.1 = ((bf16[16,24,128]{2,1,0:T(8,128)(2,1)}), bf16[16,24,128]{2,1,0:T(8,128)(2,1)S(1)}, u32[]{:S(2)}, u32[]{:S(2)}) async-start(bf16[16,24,128]{2,1,0:T(8,128)(2,1)} %sum_and_spread.1), calls=%async_computation.1 | async-start | bytes 196608 | tf_op jit(solution)/shard_map/all_to_all | solution.py:385
  34.2 1.1 %copy-start.1 = (bf16[1,192,2048]{2,1,0:T(8,128)(2,1)S(1)}, bf16[1,192,2048]{2,1,0:T(8,128)(2,1)}, u32[]{:S(2)}) copy-start(bf16[1,192,2048]{2,1,0:T(8,128)(2,1)} %param.17) | copy-start | bytes 2359300
  35.3 1.2 %copy-start.2 = (bf16[2048,256]{1,0:T(8,128)(2,1)S(1)}, bf16[2048,256]{1,0:T(8,128)(2,1)}, u32[]{:S(2)}) copy-start(bf16[2048,256]{1,0:T(8,128)(2,1)} %w_query.1) | copy-start | bytes 3145732
  36.5 1.2 %copy-start.3 = (bf16[2048,256]{1,0:T(8,128)(2,1)S(1)}, bf16[2048,256]{1,0:T(8,128)(2,1)}, u32[]{:S(2)}) copy-start(bf16[2048,256]{1,0:T(8,128)(2,1)} %w_key.1) | copy-start | bytes 3145732
  37.7 1.2 %copy-start.4 = (bf16[2048,256]{1,0:T(8,128)(2,1)S(1)}, bf16[2048,256]{1,0:T(8,128)(2,1)}, u32[]{:S(2)}) copy-start(bf16[2048,256]{1,0:T(8,128)(2,1)} %w_value.1) | copy-start | bytes 3145732
  39.0 1.2 %copy-start.5 = (bf16[2048,256]{1,0:T(8,128)(2,1)S(1)}, bf16[2048,256]{1,0:T(8,128)(2,1)}, u32[]{:S(2)}) copy-start(bf16[2048,256]{1,0:T(8,128)(2,1)} %w_gate.1) | copy-start | bytes 3145732
  40.2 0.8 copy-start.7
  42.7 52.1 %copy-start = (bf16[1024,2048]{1,0:T(8,128)(2,1)S(1)}, bf16[1024,2048]{1,0:T(8,128)(2,1)}, u32[]{:S(2)}) copy-start(bf16[1024,2048]{1,0:T(8,128)(2,1)} %w_out.1) | copy-start | bytes 12582916
  42.8 52.1 %copy-start.10 = (bf16[128]{0:T(256)(128)(2,1)S(1)}, bf16[128]{0:T(256)(128)(2,1)}, u32[]{:S(2)}) copy-start(bf16[128]{0:T(256)(128)(2,1)} %param.32) | copy-start | bytes 772
where the time goes:
time: 97.4 us; the launch traced here: 96.5 us
  blocking collectives  45.3 us (47%)
  starting transfers between devices  15.9 us (16%)
  local copies, waits for them, and re-layouts  13.4 us (14%)
  Pallas kernels  11.6 us (12%)
  waiting for transfers between devices  10.1 us (10%)
    all_to_all x3, blocking collectives, swap(): return lax.all_to_all(array, axes, 0, 0, tiled=True)  45.3 us
    all_to_all x2, starting transfers between devices, swap(): return lax.all_to_all(array, axes, 0, 0, tiled=True)  15.9 us
    all_to_all x2, waiting for transfers between devices, swap(): return lax.all_to_all(array, axes, 0, 0, tiled=True)  10.1 us
    unnamed x22, local copies, waits for them, and re-layouts  9.04 us
    pallas_call x1, Pallas kernels, on_device(): call(token_maps, 'token_maps', 1, [shape((8, Z_ROWS, 256)), shape((ROW_OF...  4.44 us
    pallas_call x1, Pallas kernels, on_device(): call(read_states, 'read_states', 4, shape((16, 72, LANES)))  2.3 us
  transfers between devices with their start and end apart: 2, of which 2 were waited for; matrix products, arithmetic and copies ran while one was open for 5% of the time, Pallas kernels for 0%

commit v1 on v0

v1 whole, which is shorter than its diff:
```python
import functools

import jax
import jax.numpy as jnp
from jax import lax
from jax.experimental import pallas as pl
from jax.experimental.pallas import tpu as pltpu
from jax.sharding import Mesh
from jax.sharding import PartitionSpec as P

D = 2048
HEAD = 128
LANES = 128
NORM_EPS = 1e-06
BETA_SCALE = 30.0

SPAN = 192
CTX_OWN = 8
ROWS = 208
CHUNK = 256
CHUNKS = 3
ROW_OF_X = 4 * SPAN

K_AT, V_AT, Q_AT, G_AT, S_AT, X_ROWS = 0, 208, 416, 608, 704, 720
C_AT, D_AT, Z_ROWS = 128, 160, 168

F32 = jnp.float32
BF16 = jnp.bfloat16


def dot(a, b, dims=((1,), (0,))):
    return lax.dot_general(a, b, (dims, ((), ())), preferred_element_type=F32)


def silu(v):
    return v / (1.0 + jnp.exp(-v))


def rounded(v):
    return v.astype(BF16).astype(F32)


def split_in_two(v):
    high = v.astype(BF16)
    return high.astype(F32), v - high.astype(F32)


def iota(shape, dim):
    return lax.broadcasted_iota(jnp.int32, shape, dim)


def fetch(pairs, sems):
    copies = [pltpu.make_async_copy(a, b, sems.at[n]) for n, (a, b) in enumerate(pairs)]
    for copy in copies:
        copy.start()
    return copies


def partial_modulation(cond_in, ctx_cond_in, w_mod_in, out, rows, cond, ctx_cond, w_mod, sems):
    pairs = ((w_mod_in, w_mod), (cond_in, cond), (ctx_cond_in, ctx_cond))
    for copy in fetch(pairs, sems):
        copy.wait()
    first = iota((8, cond.shape[1]), 0) == 0
    values = jnp.where(first, cond[...].astype(F32), ctx_cond[...].astype(F32))
    product = dot(silu(values).astype(BF16), w_mod[...])
    for r in range(2):
        for c in range(12):
            rows[r * 12 + c : r * 12 + c + 1, :] = product[r : r + 1, c * LANES : (c + 1) * LANES]
    value = rows[...].astype(BF16)
    for k in range(out.shape[0]):
        out[k] = value


def sum_and_spread(parts, out):
    total = parts[0].astype(F32)
    for k in range(1, parts.shape[0]):
        total = total + parts[k].astype(F32)
    value = total.astype(BF16)
    for k in range(out.shape[0]):
        out[k] = value


def modulated(values, gain, mods, which):
    scale = lax.rsqrt(jnp.mean(values * values, axis=-1, keepdims=True) + NORM_EPS)

    def row(block):
        at = (block // 12) * 24 + which * 12 + block % 12
        return mods[at : at + 1, :]

    out = []
    for j in range(D // LANES):
        cols = slice(j * LANES, (j + 1) * LANES)
        factor = gain[j : j + 1, :].astype(F32) * (1.0 + row(16 + j))
        out.append((values[:, cols] * scale * factor + row(j)).astype(BF16))
    return out


def project(
    parts, gain_in, decay_in, beta_in, rate_in, bias_in, extra_in, latent_in, context_in,
    w_key_in, w_value_in, w_query_in, w_gate_in, out, gate_out,
    gain, w_decay, w_beta, rate_at, bias_at, extra, latent, context, w_key, w_value, w_query,
    w_gate, sems, mods, rows_in,
):
    copies = fetch(
        (
            (latent_in, latent), (context_in, context), (gain_in, gain), (decay_in, w_decay),
            (beta_in, w_beta), (rate_in, rate_at), (bias_in, bias_at), (extra_in, extra),
            (w_key_in, w_key), (w_value_in, w_value), (w_query_in, w_query), (w_gate_in, w_gate),
        ),
        sems,
    )
    for y in range(4):
        total = parts[y].astype(F32)
        for x in range(1, 4):
            total = total + parts[4 * x + y].astype(F32)
        mods[24 * y : 24 * y + 24, :] = total
    for j in range(16):
        block = 32 + j
        at = (block // 12) * 24 + block % 12
        gate_out[j : j + 1, :] = mods[at : at + 1, :]
    for copy in copies[:8]:
        copy.wait()
    for g in range(0, SPAN, 64):
        for j, tile in enumerate(modulated(latent[0, g : g + 64, :].astype(F32), gain, mods, 0)):
            rows_in[g : g + 64, j * LANES : (j + 1) * LANES] = tile
    ctx_values = jnp.concatenate(
        [context[0].astype(F32), jnp.zeros((ROWS - SPAN - CTX_OWN, D), F32)], axis=0
    )
    for j, tile in enumerate(modulated(ctx_values, gain, mods, 1)):
        rows_in[SPAN:ROWS, j * LANES : (j + 1) * LANES] = tile
    inputs = rows_in[...]

    def heads(values):
        return [values[:, h * HEAD : (h + 1) * HEAD] for h in range(2)]

    def column(at):
        row = iota((4, 1), 0)
        value = jnp.where(row == 0, at[0, 0], at[0, 1])
        return jnp.where(row < 2, value, jnp.where(row == 2, at[1, 0], at[1, 1]))

    w_small = jnp.concatenate(
        [w[d].astype(F32) for w in (w_decay, w_beta) for d in range(2)], axis=0
    ).astype(BF16)
    rate, bias = column(rate_at), column(bias_at)
    small = rounded(dot(w_small, inputs, ((1,), (1,))))
    decay_raw, beta_raw = small[:4], small[4:]
    pre = decay_raw + bias
    soft = jnp.maximum(pre, 0.0) + jnp.log1p(jnp.exp(-jnp.abs(pre)))
    latent_only = jnp.concatenate([extra[0, 0], extra[0, 1]], axis=0)
    added = jnp.concatenate([latent_only, jnp.zeros((4, ROWS - SPAN), F32)], axis=1)
    log_decay = -rate * soft + added
    beta = BETA_SCALE * rate / (1.0 + jnp.exp(-beta_raw))
    pad = jnp.zeros((4, 256 - ROWS), F32)
    g_high, g_low = split_in_two(jnp.concatenate([log_decay, pad], axis=1))
    b_high, b_low = split_in_two(jnp.concatenate([beta, pad], axis=1))

    def unit(v):
        return v * lax.rsqrt(jnp.sum(v * v, axis=-1, keepdims=True) + NORM_EPS)

    copies[8].wait()
    keys = heads(silu(rounded(dot(inputs, w_key[...]))))
    copies[9].wait()
    values = heads(silu(rounded(dot(inputs, w_value[...]))))
    copies[10].wait()
    queries = heads(silu(rounded(dot(inputs[:SPAN], w_query[...]))))
    copies[11].wait()
    gates = heads(silu(rounded(dot(inputs[:SPAN], w_gate[...]))))
    low_lanes = iota((24, LANES), 1) < 64
    for h in range(2):
        key = unit(keys[h]).astype(BF16)
        value = values[h].astype(BF16)
        query = (unit(queries[h]) * HEAD**-0.5).astype(BF16)
        for d in range(2):
            peer = 2 * h + d
            out[peer, K_AT:V_AT, :] = key
            out[peer, V_AT:Q_AT, :] = value
            out[peer, Q_AT:G_AT, :] = query
            packed = []
            for y in range(4):
                one = gates[h][48 * y : 48 * y + 24]
                two = gates[h][48 * y + 24 : 48 * y + 48]
                if d == 0:
                    packed.append(jnp.where(low_lanes, one, pltpu.roll(two, 64, 1)))
                else:
                    packed.append(jnp.where(low_lanes, pltpu.roll(one, 64, 1), two))
            out[peer, G_AT:S_AT, :] = jnp.concatenate(packed, axis=0).astype(BF16)
            at = 2 * d + h
            four = jnp.concatenate(
                [g_high[at : at + 1], g_low[at : at + 1], b_high[at : at + 1], b_low[at : at + 1],
                 jnp.zeros((4, 256), F32)],
                axis=0,
            )
            out[peer, S_AT:X_ROWS, :] = jnp.concatenate(
                [four[:, :LANES], four[:, LANES:]], axis=0
            ).astype(BF16)


def unit_inverses(lows, depths, starts=None):
    width, results = (1, [None] * len(lows)) if starts is None else starts
    while width < max(depths):
        inner = [None] * len(lows)
        for n, low in enumerate(lows):
            if width >= depths[n]:
                continue
            i, j = iota(low.shape, 0), iota(low.shape, 1)
            coupled = (i // (2 * width) == j // (2 * width)) & (i // width != j // width)
            coupling = jnp.where(coupled, low, 0.0)
            if width == 1:
                results[n] = jnp.where(i == j, 1.0, 0.0) - coupling
            else:
                inner[n] = (dot(coupling.astype(BF16), results[n].astype(BF16))).astype(BF16)
        for n in range(len(lows)):
            if inner[n] is not None:
                results[n] = results[n] - dot(results[n].astype(BF16), inner[n])
        width *= 2
    return results


class Order:
    def __init__(self):
        self.backward = lax.rem(lax.axis_index("x"), 2)
        sign = 1 - 2 * self.backward
        self.ahead = sign * (iota((CHUNK, CHUNK), 0) - iota((CHUNK, CHUNK), 1))
        self.upto = jnp.where(self.ahead >= 0, 1.0, 0.0).astype(BF16)
        self.same = jnp.where(self.ahead == 0, 1.0, 0.0).astype(BF16)

    def at(self, step, count):
        return jnp.where(self.backward == 0, step, count - 1 - step)

    def block(self, key, rows):
        n = key.shape[0]
        sums = dot(self.upto[:n, :n], rows, ((1,), (1,)))
        rates = dot(self.same[:n, :n], rows, ((1,), (1,)))
        down = sums[:, 0:1] + sums[:, 1:2]
        beta = rates[:, 2:3] + rates[:, 3:4]
        across = dot(rows, self.upto[:n, :n], ((1,), (1,)))
        along = across[0:1] + across[1:2]
        reach = self.ahead[:n, :n]
        weights = jnp.where(reach >= 0, jnp.exp(jnp.where(reach >= 0, down - along, 0.0)), 0.0)
        total = jnp.where(self.backward == 0, down[n - 1 : n], down[0:1])
        low = jnp.where(reach > 0, dot(key, key, ((1,), (1,))) * weights * beta, 0.0)
        kept = (key.astype(F32) * jnp.exp(total - down)).astype(BF16)
        return low, beta, jnp.exp(down), weights, kept, jnp.exp(total)


def token_maps(got, out, reads, offsets, maps, queries):
    order = Order()
    low_lanes = iota((8, LANES), 1) < 64

    small = [got[p, S_AT:X_ROWS, :].astype(F32) for p in range(4)]
    first = [s[:8] for s in small]
    second = [s[8:] for s in small]
    turn = lambda v: pltpu.roll(v, 64, 1)
    blocks = [
        first[0],
        jnp.where(low_lanes, second[0], turn(first[1])),
        jnp.where(low_lanes, turn(first[1]), turn(second[1])),
        first[2],
        jnp.where(low_lanes, second[2], turn(first[3])),
        jnp.where(low_lanes, turn(first[3]), turn(second[3])),
    ]
    lane = iota((8, LANES), 1)
    ctx_small = jnp.zeros((8, LANES), F32)
    for p in range(4):
        here = (lane >= 8 * p) & (lane < 8 * p + 8)
        ctx_small = jnp.where(here, pltpu.roll(second[p], (64 + 8 * p) % 128, 1), ctx_small)
    ctx_small = ctx_small.astype(BF16)

    def latent_rows(at, m):
        pieces = {
            0: ((0, 0, 192), (1, 0, 64)),
            1: ((1, 64, 192), (2, 0, 128)),
            2: ((2, 128, 192), (3, 0, 192)),
        }[m]
        return jnp.concatenate([got[p, at + a : at + b, :] for p, a, b in pieces], axis=0)

    def ctx_rows(at):
        return jnp.concatenate(
            [got[p, at + SPAN : at + ROWS, :].astype(F32)[:CTX_OWN] for p in range(4)], axis=0
        ).astype(BF16)

    keys = [latent_rows(K_AT, m) for m in range(CHUNKS)]
    rows = [
        jnp.concatenate([blocks[2 * m], blocks[2 * m + 1]], axis=1).astype(BF16)
        for m in range(CHUNKS)
    ]
    ctx_key = ctx_rows(K_AT)
    padded = jnp.concatenate([ctx_key, jnp.zeros((LANES - 32, HEAD), BF16)], axis=0)
    found = [order.block(k, r) for k, r in zip(keys, rows)]
    ctx_low = order.block(padded, ctx_small)[0]
    inverses = unit_inverses([f[0] for f in found] + [ctx_low], [CHUNK] * CHUNKS + [32])
    factors = []
    for m, (_, beta, decayed, _, _, _) in enumerate(found):
        value = (latent_rows(V_AT, m).astype(F32) * beta).astype(BF16)
        key = (keys[m].astype(F32) * (beta * decayed)).astype(BF16)
        factors.append(
            dot(inverses[m].astype(BF16), jnp.concatenate([value, key], axis=1)).astype(BF16)
        )

    unit = jnp.where(iota((HEAD, HEAD), 0) == iota((HEAD, HEAD), 1), 1.0, 0.0)
    for m, (_, _, _, _, kept, total) in enumerate(found):
        both = dot(kept, factors[m], ((0,), (0,)))
        maps[m] = jnp.concatenate([both[:, :HEAD], total * unit - both[:, HEAD:]], axis=1)
    for m, (_, _, decayed, weights, _, _) in enumerate(found):
        query = latent_rows(Q_AT, m)
        pairs = (dot(query, keys[m], ((1,), (1,))) * weights).astype(BF16)
        local = dot(pairs, factors[m])
        queries[m] = jnp.concatenate(
            [local[:, :HEAD], query.astype(F32) * decayed - local[:, HEAD:]], axis=1
        )
    so_far = None
    for step in range(CHUNKS):
        m = order.at(step, CHUNKS)
        here = queries[m]
        at = pl.ds(pl.multiple_of(m * CHUNK, CHUNK), CHUNK)
        if step == 0:
            reads[at, :] = here[:, HEAD:].astype(BF16)
            offsets[at, :] = here[:, :HEAD]
            so_far = maps[m]
        else:
            moved = dot(here[:, HEAD:].astype(BF16), so_far.astype(BF16))
            reads[at, :] = moved[:, HEAD:].astype(BF16)
            offsets[at, :] = here[:, :HEAD] + moved[:, :HEAD]
            mine = maps[m]
            nxt = dot(mine[:, HEAD:].astype(BF16), so_far.astype(BF16))
            so_far = jnp.concatenate([nxt[:, :HEAD] + mine[:, :HEAD], nxt[:, HEAD:]], axis=1)
    whole = so_far.astype(BF16)
    tokens = jnp.concatenate([ctx_key, ctx_rows(V_AT)], axis=1)
    inverse = inverses[CHUNKS]
    packed = inverse[:8]
    for r in range(1, 4):
        packed = jnp.where(
            lane // 32 == r, pltpu.roll(inverse[8 * r : 8 * r + 8], 32 * r, 1), packed
        )
    tail = jnp.concatenate([packed, ctx_small.astype(F32)], axis=1).astype(BF16)
    for k in range(out.shape[0]):
        out[k, :C_AT, :] = whole
        out[k, C_AT:D_AT, :] = tokens
        out[k, D_AT:, :] = tail


def read_states(got, reads, offsets, sent, out):
    order = Order()
    count = got.shape[0]
    before = order.at(lax.axis_index("z"), count)
    unit = jnp.where(iota((HEAD, HEAD), 0) == iota((HEAD, HEAD), 1), 1.0, 0.0)

    key = jnp.concatenate([got[k, C_AT:D_AT, :HEAD] for k in range(count)], axis=0)
    value = jnp.concatenate([got[k, C_AT:D_AT, HEAD:] for k in range(count)], axis=0)
    lane = iota((8, LANES), 1)
    rows = [jnp.zeros((8, LANES), F32)] * 2
    blocks = []
    for k in range(count):
        tail = got[k, D_AT:, :].astype(F32)
        here = lane // 32 == k % 4
        rows[k // 4] = jnp.where(here, pltpu.roll(tail[:, LANES:], 32 * (k % 4), 1), rows[k // 4])
        for r in range(4):
            turned = pltpu.roll(tail[:, :LANES], (32 * (k % 4 - r)) % LANES, 1)
            one = jnp.where(here, turned, 0.0)
            none = jnp.zeros((8, LANES), F32)
            blocks.append(jnp.concatenate([one, none] if k < 4 else [none, one], axis=1))
    start = jnp.concatenate(blocks, axis=0)
    low, beta, _, _, kept, _ = order.block(key, jnp.concatenate(rows, axis=1).astype(BF16))
    inverse = unit_inverses([low], [CHUNK], (32, [start]))[0]
    fresh = dot(inverse.astype(BF16), (value.astype(F32) * beta).astype(BF16))
    ctx_state = dot(kept, fresh.astype(BF16), ((0,), (0,)))

    chain = jnp.concatenate([jnp.zeros((HEAD, HEAD), F32), unit], axis=1)
    for step in range(count - 1):
        mine = got[order.at(step, count), :C_AT, :]
        nxt = dot(mine[:, HEAD:], chain.astype(BF16))
        nxt = jnp.concatenate([nxt[:, :HEAD] + mine[:, :HEAD].astype(F32), nxt[:, HEAD:]], axis=1)
        chain = jnp.where(step < before, nxt, chain)
    state = dot(chain[:, HEAD:].astype(BF16), ctx_state.astype(BF16)) + chain[:, :HEAD]
    state = state.astype(BF16)
    for x in range(4):
        at = slice(SPAN * x, SPAN * x + SPAN)
        o = dot(reads[at, :], state) + offsets[at, :]
        gates = sent[x, G_AT:S_AT, :].astype(F32)
        for y in range(4):
            out[4 * x + y] = jnp.concatenate(
                [o[48 * y : 48 * y + 48], gates[24 * y : 24 * y + 24]], axis=0
            ).astype(BF16)


def mix(got, out_gain, gate, w_out, latent, out):
    low_lanes = iota((24, LANES), 1) < 64
    gain = out_gain[...].astype(F32)
    tiles = []
    for y in range(4):
        for h in range(2):
            one = got[8 * h + y].astype(F32)
            two = got[8 * h + 4 + y].astype(F32)
            o = one[:48] + two[:48]
            one, two = one[48:], two[48:]
            gates = jnp.concatenate(
                [
                    jnp.where(low_lanes, one, pltpu.roll(two, 64, 1)),
                    jnp.where(low_lanes, pltpu.roll(one, 64, 1), two),
                ],
                axis=0,
            )
            normed = o * lax.rsqrt(jnp.mean(o * o, axis=-1, keepdims=True) + NORM_EPS)
            tiles.append((normed * gain * gates).astype(BF16))
    gated = jnp.concatenate(tiles, axis=1)
    start = pl.multiple_of(lax.axis_index("tp") * 48, 16)
    own = latent[pl.ds(start, 48), :].astype(F32)
    for n in range(0, D, 512):
        mixed = dot(gated, w_out[:, n : n + 512])
        for c in range(0, 512, LANES):
            j = (n + c) // LANES
            cols = slice(n + c, n + c + LANES)
            out[:, cols] = (own[:, cols] + gate[j : j + 1, :] * mixed[:, c : c + LANES]).astype(BF16)


VM = pl.BlockSpec(memory_space=pltpu.VMEM)


HBM = pl.BlockSpec(memory_space=pltpu.HBM)


def call(body, name, n_in, outs, scratch=(), mib=16, n_hbm=0):
    many = isinstance(outs, (list, tuple))
    return pl.pallas_call(
        body,
        out_shape=outs,
        in_specs=[VM] * n_in + [HBM] * n_hbm,
        out_specs=[VM] * len(outs) if many else VM,
        scratch_shapes=list(scratch),
        compiler_params=pltpu.CompilerParams(vmem_limit_bytes=mib << 20),
        name=name,
    )


def shape(dims, dtype=BF16):
    return jax.ShapeDtypeStruct(dims, dtype)


def swap(array, axes):
    return lax.all_to_all(array, axes, 0, 0, tiled=True)


def on_device(
    latent, cond, context, ctx_cond, w_mod, norm_gain, w_query, w_key, w_value, w_outgate,
    w_decay, w_beta, decay_rate, decay_bias, extra_decay, out_gain, w_out,
):
    partial = call(
        partial_modulation, "partial_modulation", 0, shape((8, 24, LANES)),
        [
            pltpu.VMEM((24, LANES), F32), pltpu.VMEM(cond.shape, BF16),
            pltpu.VMEM(cond.shape, BF16), pltpu.VMEM(w_mod.shape, BF16),
            pltpu.SemaphoreType.DMA((3,)),
        ],
        58, 3,
    )(cond, ctx_cond[None, :], w_mod)
    summed = call(sum_and_spread, "sum_and_spread", 1, shape((16, 24, LANES)))(swap(partial, "z"))
    parts = swap(summed, ("x", "tp"))
    by_row = lambda w: w.transpose(1, 2, 0)
    fetched = (
        norm_gain.reshape(16, LANES), by_row(w_decay), by_row(w_beta), decay_rate, decay_bias,
        extra_decay, latent, context, w_key, w_value, w_query, w_outgate,
    )
    space = lambda n: pltpu.SMEM if n in (3, 4) else pltpu.VMEM
    sent, gate = call(
        project, "project", 1, [shape((4, X_ROWS, LANES)), shape((16, LANES), F32)],
        [space(n)(a.shape, a.dtype) for n, a in enumerate(fetched)]
        + [
            pltpu.SemaphoreType.DMA((len(fetched),)), pltpu.VMEM((96, LANES), F32),
            pltpu.VMEM((ROWS, D), BF16),
        ],
        58, len(fetched),
    )(parts, *fetched)
    held = swap(sent, "x")
    maps, reads, offsets = call(
        token_maps, "token_maps", 1,
        [shape((8, Z_ROWS, 256)), shape((ROW_OF_X, HEAD)), shape((ROW_OF_X, HEAD), F32)],
        [pltpu.VMEM((CHUNKS, HEAD, 256), F32), pltpu.VMEM((CHUNKS, CHUNK, 256), F32)],
    )(held)
    reached = swap(maps, "z")
    outs = call(read_states, "read_states", 4, shape((16, 72, LANES)))(
        reached, reads, offsets, held
    )
    own = swap(outs, ("x", "tp"))
    mixed = call(mix, "mix", 5, shape((48, D)))(own, out_gain[None, :], gate, w_out, latent[0])
    return mixed[None]


def solution(mesh):
    torus = Mesh(
        mesh.devices.reshape(8, 4, mesh.shape["tp"], mesh.shape["dp"]), ("z", "x", "tp", "dp")
    )
    sp = ("z", "x")
    return jax.shard_map(
        on_device,
        mesh=torus,
        in_specs=(
            P("dp", sp, None),
            P("dp", sp),
            P("dp", sp, None),
            P(sp),
            P(sp, "tp"),
            P(),
            P(None, "tp"),
            P(None, "tp"),
            P(None, "tp"),
            P(None, "tp"),
            P(None, None, "tp"),
            P(None, None, "tp"),
            P(None, "tp"),
            P(None, "tp"),
            P("dp", None, "tp", sp),
            P(),
            P(),
        ),
        out_specs=P("dp", ("z", "x", "tp"), None),
        check_vma=False,
    )
```

time: 97.4 us -> 92.1 us (0.946)
  blocking collectives: 45.3 us -> 74.7 us
  starting transfers between devices: 15.9 us -> 0 us
  local copies, waits for them, and re-layouts: 13.4 us -> 0.03 us
  waiting for transfers between devices: 10.1 us -> 0 us
  Pallas kernels: 11.6 us -> 16.9 us
    all_to_all x3 -> x5, blocking collectives: 45.3 us -> 74.7 us  [swap(): return lax.all_to_all(array, axes, 0, 0, tiled=True)]
    all_to_all x2 -> x0, starting transfers between devices: 15.9 us -> none  [swap(): return lax.all_to_all(array, axes, 0, 0, tiled=True)]
    all_to_all x2 -> x0, waiting for transfers between devices: 10.1 us -> none  [swap(): return lax.all_to_all(array, axes, 0, 0, tiled=True)]
    unnamed x22 -> x8, local copies, waits for them, and re-layouts: 9.04 us -> 0.03 us
    pallas_call x2, Pallas kernels: 2.58 us -> 7.91 us  [the longest x1 6.16 us: on_device(): call(project, 'project', 1, [shape((4, X_ROWS, LANES)), shape((16, LANES)...]
    reshape x5 -> x0, local copies, waits for them, and re-layouts: 3.68 us -> none  [the longest x1 0.76 us: on_device(): decay_rate.reshape(4, 1)]
  transfers between devices with their start and end apart: 2 -> 0, of which waited for: 2 -> 0; matrix products, arithmetic and copies ran while one was open for 5% -> 0% of each run, Pallas kernels for 0% -> 0%
where the time goes in v1:
time: 92.1 us; the launch traced here: 91.6 us
  blocking collectives  74.7 us (81%)
  Pallas kernels  16.9 us (18%)
    all_to_all x5, blocking collectives, swap(): return lax.all_to_all(array, axes, 0, 0, tiled=True)  74.7 us
    pallas_call x1, Pallas kernels, on_device(): call(project, 'project', 1, [shape((4, X_ROWS, LANES)), shape((16, LANES)...  6.16 us
    pallas_call x1, Pallas kernels, on_device(): call(token_maps, 'token_maps', 1, [shape((8, Z_ROWS, 256)), shape((ROW_OF...  4.41 us
    pallas_call x1, Pallas kernels, on_device(): call(read_states, 'read_states', 4, shape((16, 72, LANES)))  2.91 us

profile of v1, /device:TPU:2, one launch (start us, length us, event | category | flops | bytes accessed | tf_op | source)
XLA Modules:
  0.0 91.6 jit_solution(5525519564252513898)
XLA Ops:
  0.0 1.7 %partial_modulation.1 = bf16[8,24,128]{2,1,0:T(8,128)(2,1)} custom-call(bf16[1,64]{1,0:T(2,128)(2,1)} %cond_in.1, bf16[1,64]{1,0:T(2,128)(2,1)} %bitcast.12, bf16[64,1536]{1,0:T(8,128)(2,1)} %w_mod_in.1), custom_call_target="tpu_custom_call" | custom-call | tf_op jit(solution)/shard_map/partial_modulation/pallas_call | solution.py:447
  1.8 16.7 %all_to_all.25.parts = bf16[8,24,128]{2,1,0:T(8,128)(2,1)S(1)} all-to-all(bf16[8,24,128]{2,1,0:T(8,128)(2,1)} %partial_modulation.1), channel_id=1, replica_groups=mesh['z'=8,'x'=4,'tp'=4,'dp'=2] {'z'}, dimensions={0} | all-to-all | bytes 98304 | tf_op jit(solution)/shard_map/all_to_all | solution.py:440
  18.5 13.7 %all_to_all.26.parts = bf16[16,24,128]{2,1,0:T(8,128)(2,1)} all-to-all(bf16[16,24,128]{2,1,0:T(8,128)(2,1)S(1)} %sum_and_spread.1), channel_id=1, replica_groups=mesh['z'=8,'x'=4,'tp'=4,'dp'=2] {'x','tp'}, dimensions={0} | all-to-all | bytes 196608 | tf_op jit(solution)/shard_map/all_to_all | solution.py:440
  32.1 6.2 %project.1 = (bf16[4,720,128]{2,1,0:T(8,128)(2,1)}, f32[16,128]{1,0:T(8,128)}) custom-call(bf16[16,24,128]{2,1,0:T(8,128)(2,1)} %all_to_all.26.parts, bf16[16,128]{1,0:T(8,128)(2,1)} %bitcast.11, bf16[2,2,2048]{2,1,0:T(2,128)(2,1)} %bitcast.9, bf16[2,2,2048]{2,1,0:T(2,128)(2,1)} %bitcast.10, f32[2,2]{1,0:T(2,128)} %rate_in.1, f32[2,2]{1,0:T(2,128)} %bias_in.1, ...), custom_call_target="tpu_custom_call" | custom-call | tf_op jit(solution)/shard_map/project/pallas_call | solution.py:464
  38.3 0.0 copy-start
  38.3 0.0 copy-start.1
  38.3 0.0 copy-start.2
  38.4 0.0 copy-start.3
  38.4 13.0 %all_to_all.27.got.sent = bf16[4,720,128]{2,1,0:T(8,128)(2,1)S(1)} all-to-all(bf16[4,720,128]{2,1,0:T(8,128)(2,1)} %get-tuple-element.10), channel_id=1, replica_groups=mesh['z'=8,'x'=4,'tp'=4,'dp'=2] {'x'}, dimensions={0} | all-to-all | bytes 1474560 | tf_op jit(solution)/shard_map/all_to_all | solution.py:440
  51.4 4.4 %token_maps.1 = (bf16[8,168,256]{2,1,0:T(8,128)(2,1)S(1)}, bf16[768,128]{1,0:T(8,128)(2,1)S(1)}, f32[768,128]{1,0:T(8,128)S(1)}) custom-call(bf16[4,720,128]{2,1,0:T(8,128)(2,1)S(1)} %all_to_all.27.got.sent), custom_call_target="tpu_custom_call" | custom-call | tf_op jit(solution)/shard_map/token_maps/pallas_call | solution.py:474
  55.8 19.7 %all_to_all.28.got = bf16[8,168,256]{2,1,0:T(8,128)(2,1)S(1)} all-to-all(bf16[8,168,256]{2,1,0:T(8,128)(2,1)S(1)} %get-tuple-element.11), channel_id=1, replica_groups=mesh['z'=8,'x'=4,'tp'=4,'dp'=2] {'z'}, dimensions={0} | all-to-all | bytes 1376256 | tf_op jit(solution)/shard_map/all_to_all | solution.py:440
  75.5 2.9 %read_states.1 = bf16[16,72,128]{2,1,0:T(8,128)(2,1)S(1)} custom-call(bf16[8,168,256]{2,1,0:T(8,128)(2,1)S(1)} %all_to_all.28.got, bf16[768,128]{1,0:T(8,128)(2,1)S(1)} %get-tuple-element.12.reads, f32[768,128]{1,0:T(8,128)S(1)} %get-tuple-element.13.offsets, bf16[4,720,128]{2,1,0:T(8,128)(2,1)S(1)} %all_to_all.27.got.sent), custom_call_target="tpu_custom_call" | custom-call | tf_op jit(solution)/shard_map/read_states/pallas_call | solution.py:480
  78.4 11.6 %all_to_all.29.got = bf16[16,72,128]{2,1,0:T(8,128)(2,1)S(1)} all-to-all(bf16[16,72,128]{2,1,0:T(8,128)(2,1)S(1)} %read_states.1), channel_id=1, replica_groups=mesh['z'=8,'x'=4,'tp'=4,'dp'=2] {'x','tp'}, dimensions={0} | all-to-all | bytes 589824 | tf_op jit(solution)/shard_map/all_to_all | solution.py:440
  90.0 0.0 copy-done
  90.0 0.0 copy-done.1
  90.0 0.0 copy-done.2
  90.0 0.0 copy-done.3
  90.0 1.6 %mix.1 = bf16[48,2048]{1,0:T(8,128)(2,1)} custom-call(bf16[16,72,128]{2,1,0:T(8,128)(2,1)S(1)} %all_to_all.29.got, bf16[1,128]{1,0:T(2,128)(2,1)S(1)} %bitcast.8, f32[16,128]{1,0:T(8,128)S(1)} %copy-done.2, bf16[1024,2048]{1,0:T(8,128)(2,1)S(1)} %copy-done, bf16[192,2048]{1,0:T(8,128)(2,1)S(1)} %bitcast.7), custom_call_target="tpu_custom_call" | custom-call | tf_op jit(solution)/shard_map/mix/pallas_call | solution.py:484
  (1 shorter events, 0.0 us)
Async XLA Ops:
  38.3 51.7 %copy-start = (bf16[1024,2048]{1,0:T(8,128)(2,1)S(1)}, bf16[1024,2048]{1,0:T(8,128)(2,1)}, u32[]{:S(2)}) copy-start(bf16[1024,2048]{1,0:T(8,128)(2,1)} %w_out.1) | copy-start | bytes 12582916
  38.3 51.7 %copy-start.1 = (bf16[1,192,2048]{2,1,0:T(8,128)(2,1)S(1)}, bf16[1,192,2048]{2,1,0:T(8,128)(2,1)}, u32[]{:S(2)}) copy-start(bf16[1,192,2048]{2,1,0:T(8,128)(2,1)} %latent_in.1) | copy-start | bytes 2359300
  38.3 51.7 %copy-start.2 = (f32[16,128]{1,0:T(8,128)S(1)}, f32[16,128]{1,0:T(8,128)}, u32[]{:S(2)}) copy-start(f32[16,128]{1,0:T(8,128)} %get-tuple-element.14.gate) | copy-start | bytes 24580
  38.4 51.6 %copy-start.3 = (bf16[128]{0:T(256)(128)(2,1)S(1)}, bf16[128]{0:T(256)(128)(2,1)}, u32[]{:S(2)}) copy-start(bf16[128]{0:T(256)(128)(2,1)} %param.32) | copy-start | bytes 772

commit v2 on v1

--- a/solution.py
+++ b/solution.py
@@ -80,74 +80,87 @@
         out[k] = value
 
 
-def modulated(values, gain, mods, which):
-    scale = lax.rsqrt(jnp.mean(values * values, axis=-1, keepdims=True) + NORM_EPS)
-
-    def row(block):
-        at = (block // 12) * 24 + which * 12 + block % 12
-        return mods[at : at + 1, :]
-
-    out = []
-    for j in range(D // LANES):
-        cols = slice(j * LANES, (j + 1) * LANES)
-        factor = gain[j : j + 1, :].astype(F32) * (1.0 + row(16 + j))
-        out.append((values[:, cols] * scale * factor + row(j)).astype(BF16))
-    return out
-
-
-def project(
-    parts, gain_in, decay_in, beta_in, rate_in, bias_in, extra_in, latent_in, context_in,
-    w_key_in, w_value_in, w_query_in, w_gate_in, out, gate_out,
-    gain, w_decay, w_beta, rate_at, bias_at, extra, latent, context, w_key, w_value, w_query,
-    w_gate, sems, mods, rows_in,
+def prepare(
+    gain_in, decay_in, beta_in, rate_in, bias_in, extra_in, latent_in, context_in,
+    w_key_in, w_value_in, w_key, w_value, latent, context, factors, gain, w_small, consts,
+    w_decay, w_beta, rate, bias, extra, sems,
 ):
     copies = fetch(
         (
             (latent_in, latent), (context_in, context), (gain_in, gain), (decay_in, w_decay),
-            (beta_in, w_beta), (rate_in, rate_at), (bias_in, bias_at), (extra_in, extra),
-            (w_key_in, w_key), (w_value_in, w_value), (w_query_in, w_query), (w_gate_in, w_gate),
+            (beta_in, w_beta), (rate_in, rate), (bias_in, bias), (extra_in, extra),
+            (w_key_in, w_key), (w_value_in, w_value),
         ),
         sems,
     )
+    for copy in copies[:8]:
+        copy.wait()
+
+    def factor(values):
+        values = values.astype(F32)
+        mean = jnp.mean(values * values, axis=-1, keepdims=True)
+        return jnp.broadcast_to(lax.rsqrt(mean + NORM_EPS), (values.shape[0], LANES))
+
+    for g in range(0, SPAN, 64):
+        factors[g : g + 64, :] = factor(latent[0, g : g + 64, :])
+    factors[SPAN : SPAN + CTX_OWN, :] = factor(context[0])
+    factors[SPAN + CTX_OWN :, :] = jnp.zeros((ROWS - SPAN - CTX_OWN, LANES), F32)
+    w_small[...] = jnp.concatenate(
+        [w[d].astype(F32) for w in (w_decay, w_beta) for d in range(2)], axis=0
+    ).astype(BF16)
+
+    def spread(at):
+        row = iota((4, 256), 0)
+        value = jnp.where(row == 0, at[0, 0], at[0, 1])
+        return jnp.where(row < 2, value, jnp.where(row == 2, at[1, 0], at[1, 1]))
+
+    latent_only = jnp.concatenate([extra[0, 0], extra[0, 1]], axis=0)
+    added = jnp.concatenate([latent_only, jnp.zeros((4, 256 - SPAN), F32)], axis=1)
+    consts[...] = jnp.concatenate(
+        [added, spread(rate), spread(bias), jnp.zeros((4, 256), F32)], axis=0
+    )
+    for copy in copies[8:]:
+        copy.wait()
+
+
+def project(
+    parts, w_key, w_value, latent, context, factors, gain, w_small, consts, w_query_in, w_gate_in,
+    out, gate_out, mods, rows_in, w_query, w_gate, sems,
+):
+    copies = fetch(((w_query_in, w_query), (w_gate_in, w_gate)), sems)
     for y in range(4):
         total = parts[y].astype(F32)
         for x in range(1, 4):
             total = total + parts[4 * x + y].astype(F32)
         mods[24 * y : 24 * y + 24, :] = total
+
+    def row(which, block):
+        at = (block // 12) * 24 + which * 12 + block % 12
+        return mods[at : at + 1, :]
+
     for j in range(16):
-        block = 32 + j
-        at = (block // 12) * 24 + block % 12
-        gate_out[j : j + 1, :] = mods[at : at + 1, :]
-    for copy in copies[:8]:
-        copy.wait()
-    for g in range(0, SPAN, 64):
-        for j, tile in enumerate(modulated(latent[0, g : g + 64, :].astype(F32), gain, mods, 0)):
-            rows_in[g : g + 64, j * LANES : (j + 1) * LANES] = tile
-    ctx_values = jnp.concatenate(
-        [context[0].astype(F32), jnp.zeros((ROWS - SPAN - CTX_OWN, D), F32)], axis=0
-    )
-    for j, tile in enumerate(modulated(ctx_values, gain, mods, 1)):
-        rows_in[SPAN:ROWS, j * LANES : (j + 1) * LANES] = tile
+        gate_out[j : j + 1, :] = row(0, 32 + j)
+    none = jnp.zeros((ROWS - SPAN - CTX_OWN, LANES), F32)
+    for which, rows in ((0, slice(0, SPAN)), (1, slice(SPAN, ROWS))):
+        for j in range(16):
+            cols = slice(j * LANES, (j + 1) * LANES)
+            if which == 0:
+                values = latent[0, :, cols].astype(F32)
+            else:
+                values = jnp.concatenate([context[0, :, cols].astype(F32), none], axis=0)
+            scale = gain[j : j + 1, :].astype(F32) * (1.0 + row(which, 16 + j))
+            tile = values * factors[rows, :] * scale + row(which, j)
+            rows_in[rows, cols] = tile.astype(BF16)
     inputs = rows_in[...]
 
     def heads(values):
         return [values[:, h * HEAD : (h + 1) * HEAD] for h in range(2)]
 
-    def column(at):
-        row = iota((4, 1), 0)
-        value = jnp.where(row == 0, at[0, 0], at[0, 1])
-        return jnp.where(row < 2, value, jnp.where(row == 2, at[1, 0], at[1, 1]))
-
-    w_small = jnp.concatenate(
-        [w[d].astype(F32) for w in (w_decay, w_beta) for d in range(2)], axis=0
-    ).astype(BF16)
-    rate, bias = column(rate_at), column(bias_at)
-    small = rounded(dot(w_small, inputs, ((1,), (1,))))
+    added, rate, bias = (consts[n : n + 4, :ROWS] for n in (0, 4, 8))
+    small = rounded(dot(w_small[...], inputs, ((1,), (1,))))
     decay_raw, beta_raw = small[:4], small[4:]
     pre = decay_raw + bias
     soft = jnp.maximum(pre, 0.0) + jnp.log1p(jnp.exp(-jnp.abs(pre)))
-    latent_only = jnp.concatenate([extra[0, 0], extra[0, 1]], axis=0)
-    added = jnp.concatenate([latent_only, jnp.zeros((4, ROWS - SPAN), F32)], axis=1)
     log_decay = -rate * soft + added
     beta = BETA_SCALE * rate / (1.0 + jnp.exp(-beta_raw))
     pad = jnp.zeros((4, 256 - ROWS), F32)
@@ -157,13 +170,11 @@
     def unit(v):
         return v * lax.rsqrt(jnp.sum(v * v, axis=-1, keepdims=True) + NORM_EPS)
 
-    copies[8].wait()
     keys = heads(silu(rounded(dot(inputs, w_key[...]))))
-    copies[9].wait()
     values = heads(silu(rounded(dot(inputs, w_value[...]))))
-    copies[10].wait()
+    copies[0].wait()
     queries = heads(silu(rounded(dot(inputs[:SPAN], w_query[...]))))
-    copies[11].wait()
+    copies[1].wait()
     gates = heads(silu(rounded(dot(inputs[:SPAN], w_gate[...]))))
     low_lanes = iota((24, LANES), 1) < 64
     for h in range(2):
@@ -227,26 +238,30 @@
     def at(self, step, count):
         return jnp.where(self.backward == 0, step, count - 1 - step)
 
-    def block(self, key, rows):
-        n = key.shape[0]
+    def decays(self, rows):
+        n = rows.shape[1]
         sums = dot(self.upto[:n, :n], rows, ((1,), (1,)))
-        rates = dot(self.same[:n, :n], rows, ((1,), (1,)))
         down = sums[:, 0:1] + sums[:, 1:2]
-        beta = rates[:, 2:3] + rates[:, 3:4]
         across = dot(rows, self.upto[:n, :n], ((1,), (1,)))
         along = across[0:1] + across[1:2]
         reach = self.ahead[:n, :n]
         weights = jnp.where(reach >= 0, jnp.exp(jnp.where(reach >= 0, down - along, 0.0)), 0.0)
+        return down, weights
+
+    def block(self, key, rows):
+        n = key.shape[0]
+        down, weights = self.decays(rows)
+        rates = dot(self.same[:n, :n], rows, ((1,), (1,)))
+        beta = rates[:, 2:3] + rates[:, 3:4]
         total = jnp.where(self.backward == 0, down[n - 1 : n], down[0:1])
+        reach = self.ahead[:n, :n]
         low = jnp.where(reach > 0, dot(key, key, ((1,), (1,))) * weights * beta, 0.0)
         kept = (key.astype(F32) * jnp.exp(total - down)).astype(BF16)
-        return low, beta, jnp.exp(down), weights, kept, jnp.exp(total)
-
-
-def token_maps(got, out, reads, offsets, maps, queries):
-    order = Order()
+        return low, beta, jnp.exp(down), kept, jnp.exp(total)
+
+
+def small_rows(got):
     low_lanes = iota((8, LANES), 1) < 64
-
     small = [got[p, S_AT:X_ROWS, :].astype(F32) for p in range(4)]
     first = [s[:8] for s in small]
     second = [s[8:] for s in small]
@@ -264,49 +279,79 @@
     for p in range(4):
         here = (lane >= 8 * p) & (lane < 8 * p + 8)
         ctx_small = jnp.where(here, pltpu.roll(second[p], (64 + 8 * p) % 128, 1), ctx_small)
-    ctx_small = ctx_small.astype(BF16)
-
-    def latent_rows(at, m):
-        pieces = {
-            0: ((0, 0, 192), (1, 0, 64)),
-            1: ((1, 64, 192), (2, 0, 128)),
-            2: ((2, 128, 192), (3, 0, 192)),
-        }[m]
-        return jnp.concatenate([got[p, at + a : at + b, :] for p, a, b in pieces], axis=0)
+    rows = [
+        jnp.concatenate([blocks[2 * m], blocks[2 * m + 1]], axis=1).astype(BF16)
+        for m in range(CHUNKS)
+    ]
+    return rows, ctx_small.astype(BF16)
+
+
+def latent_rows(got, at, m):
+    pieces = {
+        0: ((0, 0, 192), (1, 0, 64)),
+        1: ((1, 64, 192), (2, 0, 128)),
+        2: ((2, 128, 192), (3, 0, 192)),
+    }[m]
+    return jnp.concatenate([got[p, at + a : at + b, :] for p, a, b in pieces], axis=0)
+
+
+def add_block(mine, so_far):
+    nxt = dot(mine[:, HEAD:].astype(BF16), so_far.astype(BF16))
+    return jnp.concatenate([nxt[:, :HEAD] + mine[:, :HEAD].astype(F32), nxt[:, HEAD:]], axis=1)
+
+
+def token_maps(got, out, reads, offsets, factors, maps, queries):
+    order = Order()
 
     def ctx_rows(at):
         return jnp.concatenate(
             [got[p, at + SPAN : at + ROWS, :].astype(F32)[:CTX_OWN] for p in range(4)], axis=0
         ).astype(BF16)
 
-    keys = [latent_rows(K_AT, m) for m in range(CHUNKS)]
-    rows = [
-        jnp.concatenate([blocks[2 * m], blocks[2 * m + 1]], axis=1).astype(BF16)
-        for m in range(CHUNKS)
-    ]
+    rows, ctx_small = small_rows(got)
+    keys = [latent_rows(got, K_AT, m) for m in range(CHUNKS)]
     ctx_key = ctx_rows(K_AT)
     padded = jnp.concatenate([ctx_key, jnp.zeros((LANES - 32, HEAD), BF16)], axis=0)
     found = [order.block(k, r) for k, r in zip(keys, rows)]
     ctx_low = order.block(padded, ctx_small)[0]
     inverses = unit_inverses([f[0] for f in found] + [ctx_low], [CHUNK] * CHUNKS + [32])
-    factors = []
-    for m, (_, beta, decayed, _, _, _) in enumerate(found):
-        value = (latent_rows(V_AT, m).astype(F32) * beta).astype(BF16)
+    for m, (_, beta, decayed, _, _) in enumerate(found):
+        value = (latent_rows(got, V_AT, m).astype(F32) * beta).astype(BF16)
         key = (keys[m].astype(F32) * (beta * decayed)).astype(BF16)
-        factors.append(
-            dot(inverses[m].astype(BF16), jnp.concatenate([value, key], axis=1)).astype(BF16)
-        )
-
+        right = jnp.concatenate([value, key], axis=1)
+        factors[m] = dot(inverses[m].astype(BF16), right).astype(BF16)
     unit = jnp.where(iota((HEAD, HEAD), 0) == iota((HEAD, HEAD), 1), 1.0, 0.0)
-    for m, (_, _, _, _, kept, total) in enumerate(found):
+    for m, (_, _, _, kept, total) in enumerate(found):
         both = dot(kept, factors[m], ((0,), (0,)))
         maps[m] = jnp.concatenate([both[:, :HEAD], total * unit - both[:, HEAD:]], axis=1)
-    for m, (_, _, decayed, weights, _, _) in enumerate(found):
-        query = latent_rows(Q_AT, m)
-        pairs = (dot(query, keys[m], ((1,), (1,))) * weights).astype(BF16)
+    so_far = maps[order.at(0, CHUNKS)]
+    for step in range(1, CHUNKS):
+        so_far = add_block(maps[order.at(step, CHUNKS)], so_far)
+    whole = so_far.astype(BF16)
+    tokens = jnp.concatenate([ctx_key, ctx_rows(V_AT)], axis=1)
+    token_reads(got, order, rows, factors, maps, reads, offsets, queries)
+    inverse = inverses[CHUNKS]
+    lane = iota((8, LANES), 1)
+    packed = inverse[:8]
+    for r in range(1, 4):
+        packed = jnp.where(
+            lane // 32 == r, pltpu.roll(inverse[8 * r : 8 * r + 8], 32 * r, 1), packed
+        )
+    tail = jnp.concatenate([packed, ctx_small.astype(F32)], axis=1).astype(BF16)
+    for k in range(out.shape[0]):
+        out[k, :C_AT, :] = whole
+        out[k, C_AT:D_AT, :] = tokens
+        out[k, D_AT:, :] = tail
+
+
+def token_reads(got, order, rows, factors, maps, reads, offsets, queries):
+    for m in range(CHUNKS):
+        down, weights = order.decays(rows[m])
+        query = latent_rows(got, Q_AT, m)
+        pairs = (dot(query, latent_rows(got, K_AT, m), ((1,), (1,))) * weights).astype(BF16)
         local = dot(pairs, factors[m])
         queries[m] = jnp.concatenate(
-            [local[:, :HEAD], query.astype(F32) * decayed - local[:, HEAD:]], axis=1
+            [local[:, :HEAD], query.astype(F32) * jnp.exp(down) - local[:, HEAD:]], axis=1
         )
     so_far = None
     for step in range(CHUNKS):
@@ -321,22 +366,8 @@
             moved = dot(here[:, HEAD:].astype(BF16), so_far.astype(BF16))
             reads[at, :] = moved[:, HEAD:].astype(BF16)
             offsets[at, :] = here[:, :HEAD] + moved[:, :HEAD]
-            mine = maps[m]
-            nxt = dot(mine[:, HEAD:].astype(BF16), so_far.astype(BF16))
-            so_far = jnp.concatenate([nxt[:, :HEAD] + mine[:, :HEAD], nxt[:, HEAD:]], axis=1)
-    whole = so_far.astype(BF16)
-    tokens = jnp.concatenate([ctx_key, ctx_rows(V_AT)], axis=1)
-    inverse = inverses[CHUNKS]
-    packed = inverse[:8]
-    for r in range(1, 4):
-        packed = jnp.where(
-            lane // 32 == r, pltpu.roll(inverse[8 * r : 8 * r + 8], 32 * r, 1), packed
-        )
-    tail = jnp.concatenate([packed, ctx_small.astype(F32)], axis=1).astype(BF16)
-    for k in range(out.shape[0]):
-        out[k, :C_AT, :] = whole
-        out[k, C_AT:D_AT, :] = tokens
-        out[k, D_AT:, :] = tail
+            if step < CHUNKS - 1:
+                so_far = add_block(maps[m], so_far)
 
 
 def read_states(got, reads, offsets, sent, out):
@@ -360,16 +391,14 @@
             none = jnp.zeros((8, LANES), F32)
             blocks.append(jnp.concatenate([one, none] if k < 4 else [none, one], axis=1))
     start = jnp.concatenate(blocks, axis=0)
-    low, beta, _, _, kept, _ = order.block(key, jnp.concatenate(rows, axis=1).astype(BF16))
+    low, beta, _, kept, _ = order.block(key, jnp.concatenate(rows, axis=1).astype(BF16))
     inverse = unit_inverses([low], [CHUNK], (32, [start]))[0]
     fresh = dot(inverse.astype(BF16), (value.astype(F32) * beta).astype(BF16))
     ctx_state = dot(kept, fresh.astype(BF16), ((0,), (0,)))
 
     chain = jnp.concatenate([jnp.zeros((HEAD, HEAD), F32), unit], axis=1)
     for step in range(count - 1):
-        mine = got[order.at(step, count), :C_AT, :]
-        nxt = dot(mine[:, HEAD:], chain.astype(BF16))
-        nxt = jnp.concatenate([nxt[:, :HEAD] + mine[:, :HEAD].astype(F32), nxt[:, HEAD:]], axis=1)
+        nxt = add_block(got[order.at(step, count), :C_AT, :], chain)
         chain = jnp.where(step < before, nxt, chain)
     state = dot(chain[:, HEAD:].astype(BF16), ctx_state.astype(BF16)) + chain[:, :HEAD]
     state = state.astype(BF16)
@@ -436,6 +465,10 @@
     return jax.ShapeDtypeStruct(dims, dtype)
 
 
+def in_hbm(array):
+    return pltpu.with_memory_space_constraint(array, pltpu.HBM)
+
+
 def swap(array, axes):
     return lax.all_to_all(array, axes, 0, 0, tiled=True)
 
@@ -444,6 +477,23 @@
     latent, cond, context, ctx_cond, w_mod, norm_gain, w_query, w_key, w_value, w_outgate,
     w_decay, w_beta, decay_rate, decay_bias, extra_decay, out_gain, w_out,
 ):
+    by_row = lambda w: w.transpose(1, 2, 0)
+    fetched = (
+        norm_gain.reshape(16, LANES), by_row(w_decay), by_row(w_beta), decay_rate, decay_bias,
+        extra_decay, latent, context, w_key, w_value,
+    )
+    space = lambda n: pltpu.SMEM if n in (3, 4) else pltpu.VMEM
+    prepared = call(
+        prepare, "prepare", 0,
+        [shape(w.shape) for w in fetched[8:]]
+        + [
+            shape(latent.shape), shape(context.shape), shape((ROWS, LANES), F32),
+            shape((16, LANES)), shape((8, D)), shape((16, 256), F32),
+        ],
+        [space(n)(a.shape, a.dtype) for n, a in enumerate(fetched) if 1 <= n <= 5]
+        + [pltpu.SemaphoreType.DMA((len(fetched),))],
+        16, len(fetched),
+    )(*(in_hbm(a) for a in fetched))
     partial = call(
         partial_modulation, "partial_modulation", 0, shape((8, 24, LANES)),
         [
@@ -451,37 +501,33 @@
             pltpu.VMEM(cond.shape, BF16), pltpu.VMEM(w_mod.shape, BF16),
             pltpu.SemaphoreType.DMA((3,)),
         ],
-        58, 3,
-    )(cond, ctx_cond[None, :], w_mod)
+        16, 3,
+    )(in_hbm(cond), in_hbm(ctx_cond[None, :]), in_hbm(w_mod))
     summed = call(sum_and_spread, "sum_and_spread", 1, shape((16, 24, LANES)))(swap(partial, "z"))
     parts = swap(summed, ("x", "tp"))
-    by_row = lambda w: w.transpose(1, 2, 0)
-    fetched = (
-        norm_gain.reshape(16, LANES), by_row(w_decay), by_row(w_beta), decay_rate, decay_bias,
-        extra_decay, latent, context, w_key, w_value, w_query, w_outgate,
-    )
-    space = lambda n: pltpu.SMEM if n in (3, 4) else pltpu.VMEM
     sent, gate = call(
-        project, "project", 1, [shape((4, X_ROWS, LANES)), shape((16, LANES), F32)],
-        [space(n)(a.shape, a.dtype) for n, a in enumerate(fetched)]
-        + [
-            pltpu.SemaphoreType.DMA((len(fetched),)), pltpu.VMEM((96, LANES), F32),
-            pltpu.VMEM((ROWS, D), BF16),
-        ],
-        58, len(fetched),
-    )(parts, *fetched)
+        project, "project", 1 + len(prepared), [shape((4, X_ROWS, LANES)), shape((16, LANES), F32)],
+        [pltpu.VMEM((96, LANES), F32), pltpu.VMEM((ROWS, D), BF16)]
+        + [pltpu.VMEM(w_query.shape, BF16)] * 2 + [pltpu.SemaphoreType.DMA((2,))],
+        24, 2,
+    )(parts, *prepared, in_hbm(w_query), in_hbm(w_outgate))
     held = swap(sent, "x")
     maps, reads, offsets = call(
         token_maps, "token_maps", 1,
         [shape((8, Z_ROWS, 256)), shape((ROW_OF_X, HEAD)), shape((ROW_OF_X, HEAD), F32)],
-        [pltpu.VMEM((CHUNKS, HEAD, 256), F32), pltpu.VMEM((CHUNKS, CHUNK, 256), F32)],
+        [
+            pltpu.VMEM((CHUNKS, CHUNK, 256), BF16), pltpu.VMEM((CHUNKS, HEAD, 256), F32),
+            pltpu.VMEM((CHUNKS, CHUNK, 256), F32),
+        ],
     )(held)
     reached = swap(maps, "z")
     outs = call(read_states, "read_states", 4, shape((16, 72, LANES)))(
         reached, reads, offsets, held
     )
-    own = swap(outs, ("x", "tp"))
-    mixed = call(mix, "mix", 5, shape((48, D)))(own, out_gain[None, :], gate, w_out, latent[0])
+    gathered = swap(outs, ("x", "tp"))
+    mixed = call(mix, "mix", 5, shape((48, D)))(
+        gathered, out_gain[None, :], gate, w_out, latent[0]
+    )
     return mixed[None]
 
 

time: 92.1 us -> 88.7 us (0.963)
  blocking collectives: 74.7 us -> 59.7 us
  starting transfers between devices: 0 us -> 7.48 us
  waiting for transfers between devices: 0 us -> 4.36 us
    all_to_all x5 -> x4, blocking collectives: 74.7 us -> 59.7 us  [swap(): return lax.all_to_all(array, axes, 0, 0, tiled=True)]
    all_to_all x0 -> x1, starting transfers between devices: none -> 7.48 us  [swap(): return lax.all_to_all(array, axes, 0, 0, tiled=True)]
    all_to_all x0 -> x1, waiting for transfers between devices: none -> 4.36 us  [swap(): return lax.all_to_all(array, axes, 0, 0, tiled=True)]
    pallas_call x1 -> x2, Pallas kernels: 6.16 us -> 5.46 us  [the longest x1 3.52 us: on_device(): call(project, 'project', 1 + len(prepared), [shape((4, X_ROWS, LANES)), s...]
  transfers between devices with their start and end apart: 0 -> 1, of which waited for: 0 -> 1; matrix products, arithmetic and copies ran while one was open for 0% -> 0% of each run, Pallas kernels for 0% -> 2%
where the time goes in v2:
time: 88.7 us; the launch traced here: 88.3 us
  blocking collectives  59.7 us (67%)
  Pallas kernels  16.7 us (19%)
  starting transfers between devices  7.48 us (8%)
  waiting for transfers between devices  4.36 us (5%)
    all_to_all x4, blocking collectives, swap(): return lax.all_to_all(array, axes, 0, 0, tiled=True)  59.7 us
    all_to_all x1, starting transfers between devices, swap(): return lax.all_to_all(array, axes, 0, 0, tiled=True)  7.48 us
    pallas_call x1, Pallas kernels, on_device(): call(token_maps, 'token_maps', 1, [shape((8, Z_ROWS, 256)), shape((ROW_OF...  4.72 us
    all_to_all x1, waiting for transfers between devices, swap(): return lax.all_to_all(array, axes, 0, 0, tiled=True)  4.36 us
    pallas_call x1, Pallas kernels, on_device(): call(project, 'project', 1 + len(prepared), [shape((4, X_ROWS, LANES)), s...  3.52 us
    pallas_call x1, Pallas kernels, on_device(): call(read_states, 'read_states', 4, shape((16, 72, LANES)))  3.09 us
    pallas_call x1, Pallas kernels, on_device(): call(prepare, 'prepare', 0, [shape(w.shape) for w in fetched[8:]] + [shap...  1.95 us
  transfers between devices with their start and end apart: 1, of which 1 were waited for; matrix products, arithmetic and copies ran while one was open for 0% of the time, Pallas kernels for 2%

profile of v2, /device:TPU:2, one launch (start us, length us, event | category | flops | bytes accessed | tf_op | source)
XLA Modules:
  0.0 88.3 jit_solution(4288221654313081078)
XLA Ops:
  0.0 1.1 %partial_modulation.1 = bf16[8,24,128]{2,1,0:T(8,128)(2,1)S(1)} custom-call(bf16[1,64]{1,0:T(2,128)(2,1)} %cond_in.1, bf16[1,64]{1,0:T(2,128)(2,1)} %bitcast.12, bf16[64,1536]{1,0:T(8,128)(2,1)} %w_mod_in.1), custom_call_target="tpu_custom_call" | custom-call | tf_op jit(solution)/shard_map/partial_modulation/pallas_call | solution.py:497
  1.1 16.5 %all_to_all.25.parts = bf16[8,24,128]{2,1,0:T(8,128)(2,1)S(1)} all-to-all(bf16[8,24,128]{2,1,0:T(8,128)(2,1)S(1)} %partial_modulation.1), channel_id=1, replica_groups=mesh['z'=8,'x'=4,'tp'=4,'dp'=2] {'z'}, dimensions={0} | all-to-all | bytes 98304 | tf_op jit(solution)/shard_map/all_to_all | solution.py:473
  17.6 0.7 sum_and_spread.1
  18.3 7.5 %all-to-all-start.1 = ((bf16[16,24,128]{2,1,0:T(8,128)(2,1)}), bf16[16,24,128]{2,1,0:T(8,128)(2,1)S(1)}, u32[]{:S(2)}, u32[]{:S(2)}) async-start(bf16[16,24,128]{2,1,0:T(8,128)(2,1)} %sum_and_spread.1), calls=%async_computation.1 | async-start | bytes 196608 | tf_op jit(solution)/shard_map/all_to_all | solution.py:473
  25.7 1.9 %prepare.1 = (bf16[2048,256]{1,0:T(8,128)(2,1)S(1)}, bf16[2048,256]{1,0:T(8,128)(2,1)S(1)}, bf16[1,192,2048]{2,1,0:T(8,128)(2,1)S(1)}, bf16[1,8,2048]{2,1,0:T(8,...) custom-call(bf16[16,128]{1,0:T(8,128)(2,1)} %bitcast.11, ...), custom_call_target="tpu_custom_call" | custom-call | tf_op jit(solution)/shard_map/prepare/pallas_call | solution.py:486
  27.7 4.4 %all-to-all-done.1.parts = bf16[16,24,128]{2,1,0:T(8,128)(2,1)S(1)} async-done(((bf16[16,24,128]{2,1,0:T(8,128)(2,1)}), bf16[16,24,128]{2,1,0:T(8,128)(2,1)S(1)}, u32[]{:S(2)}, u32[]{:S(2)}) %all-to-all-start.1) | async-done | bytes 98336 | tf_op jit(solution)/shard_map/all_to_all | solution.py:473
  32.1 3.5 %project.1 = (bf16[4,720,128]{2,1,0:T(8,128)(2,1)S(1)}, f32[16,128]{1,0:T(8,128)S(1)}) custom-call(bf16[16,24,128]{2,1,0:T(8,128)(2,1)S(1)} %all-to-all-done.1.parts, bf16[2048,256]{1,0:T(8,128)(2,1)S(1)} %get-tuple-element.18.w_key, bf16[2048,256]{1,0:T(8,128)(2,1)S(1)} %get-tuple-element.19.w_value, bf16[1,192,2048]{2,1,0:T(8,128)(2,1)S(1)} %get-tuple-element.20.latent, ...), custom_call_target="tpu_custom_call" | custom-call | tf_op jit(solution)/shard_map/project/pallas_call | solution.py:508
  35.6 0.0 copy-start
  35.6 0.0 copy-start.1
  35.6 0.0 copy-start.2
  35.6 11.9 %all_to_all.26.got.sent = bf16[4,720,128]{2,1,0:T(8,128)(2,1)S(1)} all-to-all(bf16[4,720,128]{2,1,0:T(8,128)(2,1)S(1)} %get-tuple-element.26), channel_id=1, replica_groups=mesh['z'=8,'x'=4,'tp'=4,'dp'=2] {'x'}, dimensions={0} | all-to-all | bytes 1474560 | tf_op jit(solution)/shard_map/all_to_all | solution.py:473
  47.6 4.7 %token_maps.1 = (bf16[8,168,256]{2,1,0:T(8,128)(2,1)S(1)}, bf16[768,128]{1,0:T(8,128)(2,1)S(1)}, f32[768,128]{1,0:T(8,128)S(1)}) custom-call(bf16[4,720,128]{2,1,0:T(8,128)(2,1)S(1)} %all_to_all.26.got.sent), custom_call_target="tpu_custom_call" | custom-call | tf_op jit(solution)/shard_map/token_maps/pallas_call | solution.py:515
  52.3 19.7 %all_to_all.27.got = bf16[8,168,256]{2,1,0:T(8,128)(2,1)S(1)} all-to-all(bf16[8,168,256]{2,1,0:T(8,128)(2,1)S(1)} %get-tuple-element.27), channel_id=1, replica_groups=mesh['z'=8,'x'=4,'tp'=4,'dp'=2] {'z'}, dimensions={0} | all-to-all | bytes 1376256 | tf_op jit(solution)/shard_map/all_to_all | solution.py:473
  72.0 3.1 %read_states.1 = bf16[16,72,128]{2,1,0:T(8,128)(2,1)S(1)} custom-call(bf16[8,168,256]{2,1,0:T(8,128)(2,1)S(1)} %all_to_all.27.got, bf16[768,128]{1,0:T(8,128)(2,1)S(1)} %get-tuple-element.28.reads, f32[768,128]{1,0:T(8,128)S(1)} %get-tuple-element.29.offsets, bf16[4,720,128]{2,1,0:T(8,128)(2,1)S(1)} %all_to_all.26.got.sent), custom_call_target="tpu_custom_call" | custom-call | tf_op jit(solution)/shard_map/read_states/pallas_call | solution.py:524
  75.1 11.6 %all_to_all.28.got = bf16[16,72,128]{2,1,0:T(8,128)(2,1)S(1)} all-to-all(bf16[16,72,128]{2,1,0:T(8,128)(2,1)S(1)} %read_states.1), channel_id=1, replica_groups=mesh['z'=8,'x'=4,'tp'=4,'dp'=2] {'x','tp'}, dimensions={0} | all-to-all | bytes 589824 | tf_op jit(solution)/shard_map/all_to_all | solution.py:473
  86.6 0.0 copy-done
  86.6 0.0 copy-done.1
  86.6 0.0 copy-done.2
  86.7 1.6 %mix.1 = bf16[48,2048]{1,0:T(8,128)(2,1)} custom-call(bf16[16,72,128]{2,1,0:T(8,128)(2,1)S(1)} %all_to_all.28.got, bf16[1,128]{1,0:T(2,128)(2,1)S(1)} %bitcast.8, f32[16,128]{1,0:T(8,128)S(1)} %get-tuple-element.30.gate, bf16[1024,2048]{1,0:T(8,128)(2,1)S(1)} %copy-done, bf16[192,2048]{1,0:T(8,128)(2,1)S(1)} %bitcast.7), custom_call_target="tpu_custom_call" | custom-call | tf_op jit(solution)/shard_map/mix/pallas_call | solution.py:528
Async XLA Ops:
  18.3 13.8 %all-to-all-start.1 = ((bf16[16,24,128]{2,1,0:T(8,128)(2,1)}), bf16[16,24,128]{2,1,0:T(8,128)(2,1)S(1)}, u32[]{:S(2)}, u32[]{:S(2)}) async-start(bf16[16,24,128]{2,1,0:T(8,128)(2,1)} %sum_and_spread.1), calls=%async_computation.1 | async-start | bytes 196608 | tf_op jit(solution)/shard_map/all_to_all | solution.py:473
  35.6 51.1 %copy-start = (bf16[1024,2048]{1,0:T(8,128)(2,1)S(1)}, bf16[1024,2048]{1,0:T(8,128)(2,1)}, u32[]{:S(2)}) copy-start(bf16[1024,2048]{1,0:T(8,128)(2,1)} %w_out.1) | copy-start | bytes 12582916
  35.6 51.1 %copy-start.1 = (bf16[1,192,2048]{2,1,0:T(8,128)(2,1)S(1)}, bf16[1,192,2048]{2,1,0:T(8,128)(2,1)}, u32[]{:S(2)}) copy-start(bf16[1,192,2048]{2,1,0:T(8,128)(2,1)} %latent_in.1) | copy-start | bytes 2359300
  35.6 51.0 %copy-start.2 = (bf16[128]{0:T(256)(128)(2,1)S(1)}, bf16[128]{0:T(256)(128)(2,1)}, u32[]{:S(2)}) copy-start(bf16[128]{0:T(256)(128)(2,1)} %param.32) | copy-start | bytes 772

commit v3 on v2

--- a/solution.py
+++ b/solution.py
@@ -21,8 +21,7 @@
 CHUNKS = 3
 ROW_OF_X = 4 * SPAN
 
-K_AT, V_AT, Q_AT, G_AT, S_AT, X_ROWS = 0, 208, 416, 608, 704, 720
-C_AT, D_AT, Z_ROWS = 128, 160, 168
+K_AT, V_AT, Q_AT, S_AT, X_ROWS = 0, 208, 416, 608, 624
 
 F32 = jnp.float32
 BF16 = jnp.bfloat16
@@ -176,88 +175,119 @@
     queries = heads(silu(rounded(dot(inputs[:SPAN], w_query[...]))))
     copies[1].wait()
     gates = heads(silu(rounded(dot(inputs[:SPAN], w_gate[...]))))
-    low_lanes = iota((24, LANES), 1) < 64
+    low_lanes = iota((ROWS, LANES), 1) < 64
     for h in range(2):
         key = unit(keys[h]).astype(BF16)
-        value = values[h].astype(BF16)
         query = (unit(queries[h]) * HEAD**-0.5).astype(BF16)
-        for d in range(2):
-            peer = 2 * h + d
+        gate = jnp.concatenate([gates[h], jnp.zeros((ROWS - SPAN, HEAD), F32)], axis=0)
+        small_parts = [v[2 * d + h : 2 * d + h + 1] for d in range(2)
+                       for v in (g_high, g_low, b_high, b_low)]
+        eight = jnp.concatenate(small_parts, axis=0)
+        eight = jnp.concatenate([eight[:, :LANES], eight[:, LANES:]], axis=0).astype(BF16)
+        for half in range(2):
+            peer = 2 * h + half
             out[peer, K_AT:V_AT, :] = key
-            out[peer, V_AT:Q_AT, :] = value
-            out[peer, Q_AT:G_AT, :] = query
-            packed = []
-            for y in range(4):
-                one = gates[h][48 * y : 48 * y + 24]
-                two = gates[h][48 * y + 24 : 48 * y + 48]
-                if d == 0:
-                    packed.append(jnp.where(low_lanes, one, pltpu.roll(two, 64, 1)))
-                else:
-                    packed.append(jnp.where(low_lanes, pltpu.roll(one, 64, 1), two))
-            out[peer, G_AT:S_AT, :] = jnp.concatenate(packed, axis=0).astype(BF16)
-            at = 2 * d + h
-            four = jnp.concatenate(
-                [g_high[at : at + 1], g_low[at : at + 1], b_high[at : at + 1], b_low[at : at + 1],
-                 jnp.zeros((4, 256), F32)],
-                axis=0,
-            )
-            out[peer, S_AT:X_ROWS, :] = jnp.concatenate(
-                [four[:, :LANES], four[:, LANES:]], axis=0
-            ).astype(BF16)
-
-
-def unit_inverses(lows, depths, starts=None):
-    width, results = (1, [None] * len(lows)) if starts is None else starts
-    while width < max(depths):
-        inner = [None] * len(lows)
-        for n, low in enumerate(lows):
-            if width >= depths[n]:
-                continue
-            i, j = iota(low.shape, 0), iota(low.shape, 1)
-            coupled = (i // (2 * width) == j // (2 * width)) & (i // width != j // width)
-            coupling = jnp.where(coupled, low, 0.0)
-            if width == 1:
-                results[n] = jnp.where(i == j, 1.0, 0.0) - coupling
+            if half == 0:
+                both = jnp.where(low_lanes, values[h], pltpu.roll(gate, 64, 1))
             else:
-                inner[n] = (dot(coupling.astype(BF16), results[n].astype(BF16))).astype(BF16)
-        for n in range(len(lows)):
-            if inner[n] is not None:
-                results[n] = results[n] - dot(results[n].astype(BF16), inner[n])
-        width *= 2
+                both = jnp.where(low_lanes, pltpu.roll(values[h], 64, 1), gate)
+            out[peer, V_AT:Q_AT, :] = both.astype(BF16)
+            out[peer, Q_AT:S_AT, :] = query
+            out[peer, S_AT:X_ROWS, :] = eight
+
+
+def blocks_apart():
+    lane = iota((64, 256), 1) // 64
+    return [jnp.where(lane == b, 1.0, 0.0).astype(BF16) for b in range(4)]
+
+
+def packed_inverses(lows):
+    i, j = iota((64, 256), 0), iota((64, 256), 1) % 64
+    lanes = blocks_apart()
+
+    def spread(x):
+        x = x.astype(BF16)
+        return jnp.concatenate([x * mask for mask in lanes], axis=0)
+
+    def times(xs, ys):
+        return [dot(x.astype(BF16), y) for x, y in zip(xs, ys)]
+
+    results = None
+    for width in (1, 4, 16):
+        coupled = (i // (4 * width) == j // (4 * width)) & (i // width != j // width)
+        rest = [jnp.where(coupled, low, 0.0) for low in lows]
+        if results is None:
+            unit = jnp.where(i == j, 1.0, 0.0)
+            moves = rest
+            first = [unit - m for m in moves]
+            squares = times(moves, [spread(m) for m in moves])
+        else:
+            moves = times(results, [spread(r) for r in rest])
+            spreads = [spread(r) for r in results]
+            squares = times(moves, [spread(m) for m in moves])
+            first = [r - p for r, p in zip(results, times(moves, spreads))]
+        second = times(squares, [spread(q) for q in first])
+        results = [q + p for q, p in zip(first, second)]
     return results
 
 
+def pack(low):
+    lane = iota((64, LANES), 1) < 64
+    tiles = []
+    for t in range(2):
+        tile = low[LANES * t : LANES * t + LANES, LANES * t : LANES * t + LANES]
+        tiles.append(jnp.where(lane, tile[:64], tile[64:]))
+    return jnp.concatenate(tiles, axis=1)
+
+
+def unpack(packed):
+    lanes = blocks_apart()
+    return jnp.concatenate([packed * mask.astype(F32) for mask in lanes], axis=0)
+
+
+def widened(results, lows, width, times):
+    i, j = iota((CHUNK, CHUNK), 0), iota((CHUNK, CHUNK), 1)
+    wide = times * width
+    coupled = (i // wide == j // wide) & (i // width != j // width)
+    half = [r.astype(BF16) for r in results]
+    moves = [
+        dot(r, jnp.where(coupled, low, 0.0).astype(BF16)).astype(BF16)
+        for r, low in zip(half, lows)
+    ]
+    squares = [dot(m, m).astype(BF16) for m in moves] if times == 4 else None
+    first = [r - dot(m, h) for r, m, h in zip(results, moves, half)]
+    if times == 2:
+        return first
+    return [q + dot(m, q.astype(BF16)) for q, m in zip(first, squares)]
+
+
 class Order:
-    def __init__(self):
-        self.backward = lax.rem(lax.axis_index("x"), 2)
-        sign = 1 - 2 * self.backward
-        self.ahead = sign * (iota((CHUNK, CHUNK), 0) - iota((CHUNK, CHUNK), 1))
-        self.upto = jnp.where(self.ahead >= 0, 1.0, 0.0).astype(BF16)
-        self.same = jnp.where(self.ahead == 0, 1.0, 0.0).astype(BF16)
-
-    def at(self, step, count):
-        return jnp.where(self.backward == 0, step, count - 1 - step)
-
-    def decays(self, rows):
-        n = rows.shape[1]
-        sums = dot(self.upto[:n, :n], rows, ((1,), (1,)))
-        down = sums[:, 0:1] + sums[:, 1:2]
-        across = dot(rows, self.upto[:n, :n], ((1,), (1,)))
-        along = across[0:1] + across[1:2]
-        reach = self.ahead[:n, :n]
-        weights = jnp.where(reach >= 0, jnp.exp(jnp.where(reach >= 0, down - along, 0.0)), 0.0)
-        return down, weights
+    def __init__(self, n):
+        self.away = iota((n, n), 0) - iota((n, n), 1)
+        self.same = jnp.where(self.away == 0, 1.0, 0.0).astype(BF16)
+        self.upto = [
+            jnp.where(a >= 0, 1.0, 0.0).astype(BF16) for a in (self.away, -self.away)
+        ]
 
     def block(self, key, rows):
         n = key.shape[0]
-        down, weights = self.decays(rows)
-        rates = dot(self.same[:n, :n], rows, ((1,), (1,)))
-        beta = rates[:, 2:3] + rates[:, 3:4]
-        total = jnp.where(self.backward == 0, down[n - 1 : n], down[0:1])
-        reach = self.ahead[:n, :n]
-        low = jnp.where(reach > 0, dot(key, key, ((1,), (1,))) * weights * beta, 0.0)
-        kept = (key.astype(F32) * jnp.exp(total - down)).astype(BF16)
-        return low, beta, jnp.exp(down), kept, jnp.exp(total)
+        pairs = dot(key, key, ((1,), (1,)))
+        rates = dot(self.same, rows, ((1,), (1,)))
+        key32 = key.astype(F32)
+        found = []
+        for d in range(2):
+            sums = dot(self.upto[d], rows, ((1,), (1,)))
+            down = sums[:, 4 * d : 4 * d + 1] + sums[:, 4 * d + 1 : 4 * d + 2]
+            across = dot(rows, self.upto[d], ((1,), (1,)))
+            along = across[4 * d : 4 * d + 1] + across[4 * d + 1 : 4 * d + 2]
+            reach = self.away if d == 0 else -self.away
+            weights = jnp.where(reach >= 0, jnp.exp(jnp.where(reach >= 0, down - along, 0.0)), 0.0)
+            beta = rates[:, 4 * d + 2 : 4 * d + 3] + rates[:, 4 * d + 3 : 4 * d + 4]
+            total = down[n - 1 : n] if d == 0 else down[0:1]
+            low = jnp.where(reach > 0, pairs * weights * beta, 0.0)
+            kept = (key32 * jnp.exp(total - down)).astype(BF16)
+            found.append((low, beta, jnp.exp(down), kept, jnp.exp(total), weights))
+        return found
 
 
 def small_rows(got):
@@ -283,7 +313,7 @@
         jnp.concatenate([blocks[2 * m], blocks[2 * m + 1]], axis=1).astype(BF16)
         for m in range(CHUNKS)
     ]
-    return rows, ctx_small.astype(BF16)
+    return rows, ctx_small
 
 
 def latent_rows(got, at, m):
@@ -300,135 +330,162 @@
     return jnp.concatenate([nxt[:, :HEAD] + mine[:, :HEAD].astype(F32), nxt[:, HEAD:]], axis=1)
 
 
-def token_maps(got, out, reads, offsets, factors, maps, queries):
-    order = Order()
+def token_maps(got, out, reads, offsets, weights_of, maps):
+    order = Order(CHUNK)
 
     def ctx_rows(at):
         return jnp.concatenate(
             [got[p, at + SPAN : at + ROWS, :].astype(F32)[:CTX_OWN] for p in range(4)], axis=0
-        ).astype(BF16)
+        )
 
     rows, ctx_small = small_rows(got)
     keys = [latent_rows(got, K_AT, m) for m in range(CHUNKS)]
-    ctx_key = ctx_rows(K_AT)
-    padded = jnp.concatenate([ctx_key, jnp.zeros((LANES - 32, HEAD), BF16)], axis=0)
-    found = [order.block(k, r) for k, r in zip(keys, rows)]
-    ctx_low = order.block(padded, ctx_small)[0]
-    inverses = unit_inverses([f[0] for f in found] + [ctx_low], [CHUNK] * CHUNKS + [32])
-    for m, (_, beta, decayed, _, _) in enumerate(found):
-        value = (latent_rows(got, V_AT, m).astype(F32) * beta).astype(BF16)
-        key = (keys[m].astype(F32) * (beta * decayed)).astype(BF16)
-        right = jnp.concatenate([value, key], axis=1)
-        factors[m] = dot(inverses[m].astype(BF16), right).astype(BF16)
+    values = [latent_rows(got, V_AT, m).astype(F32) for m in range(CHUNKS)]
+    ctx_key, ctx_value = ctx_rows(K_AT), ctx_rows(V_AT)
+    padded = jnp.concatenate([ctx_key, jnp.zeros((LANES - 32, HEAD), F32)], axis=0).astype(BF16)
+    ctx_lows = [f[0] for f in Order(LANES).block(padded, ctx_small.astype(BF16))]
+    left = iota((64, LANES), 1) < 64
+    ctx_low = jnp.concatenate(
+        [
+            jnp.where(left, ctx_lows[0][:64], pltpu.roll(ctx_lows[1][:64], 64, 1)),
+            jnp.zeros((64, LANES), F32),
+        ],
+        axis=1,
+    )
+    lows, rights, kept, totals, decays = [], [], [], [], []
+    for m in range(CHUNKS):
+        for d, (low, beta, decayed, keep, total, weights) in enumerate(
+            order.block(keys[m], rows[m])
+        ):
+            lows.append(low)
+            key = keys[m].astype(F32) * (beta * decayed)
+            rights.append(jnp.concatenate([values[m] * beta, key], axis=1).astype(BF16))
+            kept.append(keep)
+            totals.append(total)
+            decays.append(decayed)
+            weights_of[2 * m + d] = weights
+    packed = packed_inverses([pack(low) for low in lows] + [ctx_low])
+    inverses = widened([unpack(p) for p in packed[:-1]], lows, 64, 4)
+    factors = [dot(t.astype(BF16), r).astype(BF16) for t, r in zip(inverses, rights)]
     unit = jnp.where(iota((HEAD, HEAD), 0) == iota((HEAD, HEAD), 1), 1.0, 0.0)
-    for m, (_, _, _, kept, total) in enumerate(found):
-        both = dot(kept, factors[m], ((0,), (0,)))
-        maps[m] = jnp.concatenate([both[:, :HEAD], total * unit - both[:, HEAD:]], axis=1)
-    so_far = maps[order.at(0, CHUNKS)]
-    for step in range(1, CHUNKS):
-        so_far = add_block(maps[order.at(step, CHUNKS)], so_far)
-    whole = so_far.astype(BF16)
-    tokens = jnp.concatenate([ctx_key, ctx_rows(V_AT)], axis=1)
-    token_reads(got, order, rows, factors, maps, reads, offsets, queries)
-    inverse = inverses[CHUNKS]
-    lane = iota((8, LANES), 1)
-    packed = inverse[:8]
-    for r in range(1, 4):
-        packed = jnp.where(
-            lane // 32 == r, pltpu.roll(inverse[8 * r : 8 * r + 8], 32 * r, 1), packed
+    for n in range(2 * CHUNKS):
+        both = dot(kept[n], factors[n], ((0,), (0,)))
+        maps[n] = jnp.concatenate([both[:, :HEAD], totals[n] * unit - both[:, HEAD:]], axis=1)
+
+    so_far = [None, None]
+    passed = [[None] * CHUNKS for _ in range(2)]
+    for step in range(CHUNKS):
+        for d in range(2):
+            m = step if d == 0 else CHUNKS - 1 - step
+            passed[d][m] = so_far[d]
+            mine = maps[2 * m + d]
+            so_far[d] = mine if step == 0 else add_block(mine, so_far[d])
+    for m in range(CHUNKS):
+        query = latent_rows(got, Q_AT, m)
+        pairs = dot(query, keys[m], ((1,), (1,)))
+        at = slice(m * CHUNK, (m + 1) * CHUNK)
+        offset = None
+        for d in range(2):
+            n = 2 * m + d
+            local = dot((pairs * weights_of[n]).astype(BF16), factors[n])
+            read = (query.astype(F32) * decays[n] - local[:, HEAD:]).astype(BF16)
+            mine = local[:, :HEAD]
+            if passed[d][m] is not None:
+                moved = dot(read, passed[d][m].astype(BF16))
+                read, mine = moved[:, HEAD:].astype(BF16), mine + moved[:, :HEAD]
+            reads[at, d * HEAD : (d + 1) * HEAD] = read
+            offset = mine if offset is None else offset + mine
+        offsets[at, :] = offset
+
+    ctx_inverse = packed[-1][:32, :LANES]
+    merged = ctx_inverse + pltpu.roll(ctx_inverse, 64, 1)
+    merged = merged - jnp.where(iota((32, LANES), 0) == iota((32, LANES), 1), 1.0, 0.0)
+    narrow = iota((16, LANES), 1) < 96
+    turn = lambda v: pltpu.roll(v, 64, 1)
+    spare = jnp.concatenate(
+        [
+            turn(ctx_key), ctx_key, turn(ctx_value), turn(ctx_small),
+            jnp.where(narrow, turn(merged[:16]), pltpu.roll(merged[16:], 96, 1)),
+            jnp.zeros((8, LANES), F32),
+        ],
+        axis=0,
+    )
+    left = iota((HEAD, LANES), 1) < 64
+    whole = [
+        jnp.concatenate([jnp.where(left, m[:, :HEAD], spare), m[:, HEAD:]], axis=1) for m in so_far
+    ]
+    place = lax.axis_index("z")
+    for k in range(out.shape[0]):
+        out[k] = jnp.where(k > place, whole[0], whole[1]).astype(BF16)
+
+
+def read_states(got, reads, offsets, sent, out):
+    count = got.shape[0]
+    place = lax.axis_index("z")
+    turn = lambda v: pltpu.roll(v, 64, 1)
+    unit = jnp.where(iota((HEAD, HEAD), 0) == iota((HEAD, HEAD), 1), 1.0, 0.0)
+    left = iota((32, LANES), 1) < 64
+    lane = iota((16, LANES), 1)
+    key, value, starts = [], [], []
+    rows = [jnp.zeros((8, LANES), F32)] * 2
+    none = jnp.zeros((16, LANES), F32)
+    for k in range(count):
+        spare = got[k, :, :LANES].astype(F32)
+        key.append(jnp.where(left, turn(spare[:32]), spare[32:64]))
+        value.append(turn(spare[64:96]))
+        here = lane // 32 == k % 4
+        at = 32 * (k % 4)
+        rows[k // 4] = jnp.where(
+            here[:8], pltpu.roll(spare[96:104], (at - 64) % LANES, 1), rows[k // 4]
         )
-    tail = jnp.concatenate([packed, ctx_small.astype(F32)], axis=1).astype(BF16)
-    for k in range(out.shape[0]):
-        out[k, :C_AT, :] = whole
-        out[k, C_AT:D_AT, :] = tokens
-        out[k, D_AT:, :] = tail
-
-
-def token_reads(got, order, rows, factors, maps, reads, offsets, queries):
-    for m in range(CHUNKS):
-        down, weights = order.decays(rows[m])
-        query = latent_rows(got, Q_AT, m)
-        pairs = (dot(query, latent_rows(got, K_AT, m), ((1,), (1,))) * weights).astype(BF16)
-        local = dot(pairs, factors[m])
-        queries[m] = jnp.concatenate(
-            [local[:, :HEAD], query.astype(F32) * jnp.exp(down) - local[:, HEAD:]], axis=1
-        )
-    so_far = None
-    for step in range(CHUNKS):
-        m = order.at(step, CHUNKS)
-        here = queries[m]
-        at = pl.ds(pl.multiple_of(m * CHUNK, CHUNK), CHUNK)
-        if step == 0:
-            reads[at, :] = here[:, HEAD:].astype(BF16)
-            offsets[at, :] = here[:, :HEAD]
-            so_far = maps[m]
-        else:
-            moved = dot(here[:, HEAD:].astype(BF16), so_far.astype(BF16))
-            reads[at, :] = moved[:, HEAD:].astype(BF16)
-            offsets[at, :] = here[:, :HEAD] + moved[:, :HEAD]
-            if step < CHUNKS - 1:
-                so_far = add_block(maps[m], so_far)
-
-
-def read_states(got, reads, offsets, sent, out):
-    order = Order()
-    count = got.shape[0]
-    before = order.at(lax.axis_index("z"), count)
-    unit = jnp.where(iota((HEAD, HEAD), 0) == iota((HEAD, HEAD), 1), 1.0, 0.0)
-
-    key = jnp.concatenate([got[k, C_AT:D_AT, :HEAD] for k in range(count)], axis=0)
-    value = jnp.concatenate([got[k, C_AT:D_AT, HEAD:] for k in range(count)], axis=0)
-    lane = iota((8, LANES), 1)
-    rows = [jnp.zeros((8, LANES), F32)] * 2
-    blocks = []
-    for k in range(count):
-        tail = got[k, D_AT:, :].astype(F32)
-        here = lane // 32 == k % 4
-        rows[k // 4] = jnp.where(here, pltpu.roll(tail[:, LANES:], 32 * (k % 4), 1), rows[k // 4])
-        for r in range(4):
-            turned = pltpu.roll(tail[:, :LANES], (32 * (k % 4 - r)) % LANES, 1)
-            one = jnp.where(here, turned, 0.0)
-            none = jnp.zeros((8, LANES), F32)
-            blocks.append(jnp.concatenate([one, none] if k < 4 else [none, one], axis=1))
-    start = jnp.concatenate(blocks, axis=0)
-    low, beta, _, kept, _ = order.block(key, jnp.concatenate(rows, axis=1).astype(BF16))
-    inverse = unit_inverses([low], [CHUNK], (32, [start]))[0]
-    fresh = dot(inverse.astype(BF16), (value.astype(F32) * beta).astype(BF16))
-    ctx_state = dot(kept, fresh.astype(BF16), ((0,), (0,)))
-
-    chain = jnp.concatenate([jnp.zeros((HEAD, HEAD), F32), unit], axis=1)
+        for shift in (64, 96):
+            one = jnp.where(here, pltpu.roll(spare[104:120], (at - shift) % LANES, 1), 0.0)
+            starts.append(jnp.concatenate([one, none] if k < 4 else [none, one], axis=1))
+    key = jnp.concatenate(key, axis=0).astype(BF16)
+    value = jnp.concatenate(value, axis=0)
+    start = jnp.concatenate(starts, axis=0)
+    order = Order(CHUNK)
+    found = order.block(key, jnp.concatenate(rows, axis=1).astype(BF16))
+    lows = [f[0] for f in found]
+    whole = jnp.where(order.away == 0, 1.0, 0.0)
+    results = [jnp.where(a > 0, start, whole) for a in (order.away, -order.away)]
+    inverses = widened(widened(results, lows, 32, 4), lows, 128, 2)
+    ctx_states = []
+    for inverse, (_, beta, _, kept, _, _) in zip(inverses, found):
+        fresh = dot(inverse.astype(BF16), (value * beta).astype(BF16))
+        ctx_states.append(dot(kept, fresh.astype(BF16), ((0,), (0,))))
+
+    chains = [jnp.concatenate([jnp.zeros((HEAD, HEAD), F32), unit], axis=1)] * 2
     for step in range(count - 1):
-        nxt = add_block(got[order.at(step, count), :C_AT, :], chain)
-        chain = jnp.where(step < before, nxt, chain)
-    state = dot(chain[:, HEAD:].astype(BF16), ctx_state.astype(BF16)) + chain[:, :HEAD]
-    state = state.astype(BF16)
+        for d in range(2):
+            k = step if d == 0 else count - 1 - step
+            used = k < place if d == 0 else k > place
+            chains[d] = jnp.where(used, add_block(got[k], chains[d]), chains[d])
+    states = [
+        (dot(c[:, HEAD:].astype(BF16), s.astype(BF16)) + c[:, :HEAD]).astype(BF16)
+        for c, s in zip(chains, ctx_states)
+    ]
+    state = jnp.concatenate(states, axis=0)
+    left = iota((48, LANES), 1) < 64
     for x in range(4):
         at = slice(SPAN * x, SPAN * x + SPAN)
         o = dot(reads[at, :], state) + offsets[at, :]
-        gates = sent[x, G_AT:S_AT, :].astype(F32)
+        gates = sent[x, V_AT : V_AT + SPAN, :].astype(F32)
         for y in range(4):
-            out[4 * x + y] = jnp.concatenate(
-                [o[48 * y : 48 * y + 48], gates[24 * y : 24 * y + 24]], axis=0
-            ).astype(BF16)
+            own = slice(48 * y, 48 * y + 48)
+            out[4 * x + y] = jnp.where(left, o[own], gates[own]).astype(BF16)
 
 
 def mix(got, out_gain, gate, w_out, latent, out):
-    low_lanes = iota((24, LANES), 1) < 64
+    left = iota((48, LANES), 1) < 64
     gain = out_gain[...].astype(F32)
     tiles = []
     for y in range(4):
         for h in range(2):
             one = got[8 * h + y].astype(F32)
             two = got[8 * h + 4 + y].astype(F32)
-            o = one[:48] + two[:48]
-            one, two = one[48:], two[48:]
-            gates = jnp.concatenate(
-                [
-                    jnp.where(low_lanes, one, pltpu.roll(two, 64, 1)),
-                    jnp.where(low_lanes, pltpu.roll(one, 64, 1), two),
-                ],
-                axis=0,
-            )
+            o = jnp.where(left, one, pltpu.roll(two, 64, 1))
+            gates = jnp.where(left, pltpu.roll(one, 64, 1), two)
             normed = o * lax.rsqrt(jnp.mean(o * o, axis=-1, keepdims=True) + NORM_EPS)
             tiles.append((normed * gain * gates).astype(BF16))
     gated = jnp.concatenate(tiles, axis=1)
@@ -514,14 +571,13 @@
     held = swap(sent, "x")
     maps, reads, offsets = call(
         token_maps, "token_maps", 1,
-        [shape((8, Z_ROWS, 256)), shape((ROW_OF_X, HEAD)), shape((ROW_OF_X, HEAD), F32)],
+        [shape((8, HEAD, 256)), shape((ROW_OF_X, 256)), shape((ROW_OF_X, HEAD), F32)],
         [
-            pltpu.VMEM((CHUNKS, CHUNK, 256), BF16), pltpu.VMEM((CHUNKS, HEAD, 256), F32),
-            pltpu.VMEM((CHUNKS, CHUNK, 256), F32),
+            pltpu.VMEM((2 * CHUNKS, CHUNK, CHUNK), F32), pltpu.VMEM((2 * CHUNKS, HEAD, 256), F32),
         ],
     )(held)
     reached = swap(maps, "z")
-    outs = call(read_states, "read_states", 4, shape((16, 72, LANES)))(
+    outs = call(read_states, "read_states", 4, shape((16, 48, LANES)))(
         reached, reads, offsets, held
     )
     gathered = swap(outs, ("x", "tp"))

time: 88.7 us -> 85.3 us (0.962)
  blocking collectives: 59.7 us -> 55 us
  Pallas kernels: 16.7 us -> 18.1 us
    all_to_all x4, blocking collectives: 59.7 us -> 55 us  [swap(): return lax.all_to_all(array, axes, 0, 0, tiled=True)]
where the time goes in v3:
time: 85.3 us; the launch traced here: 85 us
  blocking collectives  55 us (64%)
  Pallas kernels  18.1 us (21%)
  starting transfers between devices  7.48 us (9%)
  waiting for transfers between devices  4.36 us (5%)
    all_to_all x4, blocking collectives, swap(): return lax.all_to_all(array, axes, 0, 0, tiled=True)  55 us
    all_to_all x1, starting transfers between devices, swap(): return lax.all_to_all(array, axes, 0, 0, tiled=True)  7.48 us
    pallas_call x1, Pallas kernels, on_device(): call(token_maps, 'token_maps', 1, [shape((8, HEAD, 256)), shape((ROW_OF_X...  5.35 us
    all_to_all x1, waiting for transfers between devices, swap(): return lax.all_to_all(array, axes, 0, 0, tiled=True)  4.36 us
    pallas_call x1, Pallas kernels, on_device(): call(project, 'project', 1 + len(prepared), [shape((4, X_ROWS, LANES)), s...  3.96 us
    pallas_call x1, Pallas kernels, on_device(): call(read_states, 'read_states', 4, shape((16, 48, LANES)))  3.24 us
    pallas_call x1, Pallas kernels, on_device(): call(prepare, 'prepare', 0, [shape(w.shape) for w in fetched[8:]] + [shap...  1.95 us
    pallas_call x1, Pallas kernels, on_device(): call(mix, 'mix', 5, shape((48, D)))  1.78 us
  transfers between devices with their start and end apart: 1, of which 1 were waited for; matrix products, arithmetic and copies ran while one was open for 0% of the time, Pallas kernels for 2%

profile of v3, /device:TPU:2, one launch (start us, length us, event | category | flops | bytes accessed | tf_op | source)
XLA Modules:
  0.0 85.0 jit_solution(6965070378319294452)
XLA Ops:
  0.0 1.1 %partial_modulation.1 = bf16[8,24,128]{2,1,0:T(8,128)(2,1)S(1)} custom-call(bf16[1,64]{1,0:T(2,128)(2,1)} %cond_in.1, bf16[1,64]{1,0:T(2,128)(2,1)} %bitcast.12, bf16[64,1536]{1,0:T(8,128)(2,1)} %w_mod_in.1), custom_call_target="tpu_custom_call" | custom-call | tf_op jit(solution)/shard_map/partial_modulation/pallas_call | solution.py:554
  1.1 16.5 %all_to_all.25.parts = bf16[8,24,128]{2,1,0:T(8,128)(2,1)S(1)} all-to-all(bf16[8,24,128]{2,1,0:T(8,128)(2,1)S(1)} %partial_modulation.1), channel_id=1, replica_groups=mesh['z'=8,'x'=4,'tp'=4,'dp'=2] {'z'}, dimensions={0} | all-to-all | bytes 98304 | tf_op jit(solution)/shard_map/all_to_all | solution.py:530
  17.6 0.7 sum_and_spread.1
  18.3 7.5 %all-to-all-start.1 = ((bf16[16,24,128]{2,1,0:T(8,128)(2,1)}), bf16[16,24,128]{2,1,0:T(8,128)(2,1)S(1)}, u32[]{:S(2)}, u32[]{:S(2)}) async-start(bf16[16,24,128]{2,1,0:T(8,128)(2,1)} %sum_and_spread.1), calls=%async_computation.1 | async-start | bytes 196608 | tf_op jit(solution)/shard_map/all_to_all | solution.py:530
  25.7 1.9 %prepare.1 = (bf16[2048,256]{1,0:T(8,128)(2,1)S(1)}, bf16[2048,256]{1,0:T(8,128)(2,1)S(1)}, bf16[1,192,2048]{2,1,0:T(8,128)(2,1)S(1)}, bf16[1,8,2048]{2,1,0:T(8,...) custom-call(bf16[16,128]{1,0:T(8,128)(2,1)} %bitcast.11, ...), custom_call_target="tpu_custom_call" | custom-call | tf_op jit(solution)/shard_map/prepare/pallas_call | solution.py:543
  27.7 4.4 %all-to-all-done.1.parts = bf16[16,24,128]{2,1,0:T(8,128)(2,1)S(1)} async-done(((bf16[16,24,128]{2,1,0:T(8,128)(2,1)}), bf16[16,24,128]{2,1,0:T(8,128)(2,1)S(1)}, u32[]{:S(2)}, u32[]{:S(2)}) %all-to-all-start.1) | async-done | bytes 98336 | tf_op jit(solution)/shard_map/all_to_all | solution.py:530
  32.1 0.0 copy-start
  32.1 0.0 copy-start.1
  32.1 0.0 copy-start.2
  32.1 4.0 %project.1 = (bf16[4,624,128]{2,1,0:T(8,128)(2,1)S(1)}, f32[16,128]{1,0:T(8,128)S(1)}) custom-call(bf16[16,24,128]{2,1,0:T(8,128)(2,1)S(1)} %all-to-all-done.1.parts, bf16[2048,256]{1,0:T(8,128)(2,1)S(1)} %get-tuple-element.18.w_key, bf16[2048,256]{1,0:T(8,128)(2,1)S(1)} %get-tuple-element.19.w_value, bf16[1,192,2048]{2,1,0:T(8,128)(2,1)S(1)} %get-tuple-element.20.latent, ...), custom_call_target="tpu_custom_call" | custom-call | tf_op jit(solution)/shard_map/project/pallas_call | solution.py:565
  36.0 11.2 %all_to_all.26.got.sent = bf16[4,624,128]{2,1,0:T(8,128)(2,1)S(1)} all-to-all(bf16[4,624,128]{2,1,0:T(8,128)(2,1)S(1)} %get-tuple-element.26), channel_id=1, replica_groups=mesh['z'=8,'x'=4,'tp'=4,'dp'=2] {'x'}, dimensions={0} | all-to-all | bytes 1277952 | tf_op jit(solution)/shard_map/all_to_all | solution.py:530
  47.2 5.4 %token_maps.1 = (bf16[8,128,256]{2,1,0:T(8,128)(2,1)S(1)}, bf16[768,256]{1,0:T(8,128)(2,1)S(1)}, f32[768,128]{1,0:T(8,128)S(1)}) custom-call(bf16[4,624,128]{2,1,0:T(8,128)(2,1)S(1)} %all_to_all.26.got.sent), custom_call_target="tpu_custom_call" | custom-call | tf_op jit(solution)/shard_map/token_maps/pallas_call | solution.py:572
  52.6 16.2 %all_to_all.27.got = bf16[8,128,256]{2,1,0:T(8,128)(2,1)S(1)} all-to-all(bf16[8,128,256]{2,1,0:T(8,128)(2,1)S(1)} %get-tuple-element.27), channel_id=1, replica_groups=mesh['z'=8,'x'=4,'tp'=4,'dp'=2] {'z'}, dimensions={0} | all-to-all | bytes 1048576 | tf_op jit(solution)/shard_map/all_to_all | solution.py:530
  68.7 3.2 %read_states.1 = bf16[16,48,128]{2,1,0:T(8,128)(2,1)S(1)} custom-call(bf16[8,128,256]{2,1,0:T(8,128)(2,1)S(1)} %all_to_all.27.got, bf16[768,256]{1,0:T(8,128)(2,1)S(1)} %get-tuple-element.28.reads, f32[768,128]{1,0:T(8,128)S(1)} %get-tuple-element.29.offsets, bf16[4,624,128]{2,1,0:T(8,128)(2,1)S(1)} %all_to_all.26.got.sent), custom_call_target="tpu_custom_call" | custom-call | tf_op jit(solution)/shard_map/read_states/pallas_call | solution.py:580
  72.0 11.2 %all_to_all.28.got = bf16[16,48,128]{2,1,0:T(8,128)(2,1)S(1)} all-to-all(bf16[16,48,128]{2,1,0:T(8,128)(2,1)S(1)} %read_states.1), channel_id=1, replica_groups=mesh['z'=8,'x'=4,'tp'=4,'dp'=2] {'x','tp'}, dimensions={0} | all-to-all | bytes 393216 | tf_op jit(solution)/shard_map/all_to_all | solution.py:530
  83.2 0.0 copy-done
  83.2 0.0 copy-done.1
  83.2 0.0 copy-done.2
  83.2 1.8 %mix.1 = bf16[48,2048]{1,0:T(8,128)(2,1)} custom-call(bf16[16,48,128]{2,1,0:T(8,128)(2,1)S(1)} %all_to_all.28.got, bf16[1,128]{1,0:T(2,128)(2,1)S(1)} %bitcast.8, f32[16,128]{1,0:T(8,128)S(1)} %get-tuple-element.30.gate, bf16[1024,2048]{1,0:T(8,128)(2,1)S(1)} %copy-done, bf16[192,2048]{1,0:T(8,128)(2,1)S(1)} %bitcast.7), custom_call_target="tpu_custom_call" | custom-call | tf_op jit(solution)/shard_map/mix/pallas_call | solution.py:584
Async XLA Ops:
  18.3 13.8 %all-to-all-start.1 = ((bf16[16,24,128]{2,1,0:T(8,128)(2,1)}), bf16[16,24,128]{2,1,0:T(8,128)(2,1)S(1)}, u32[]{:S(2)}, u32[]{:S(2)}) async-start(bf16[16,24,128]{2,1,0:T(8,128)(2,1)} %sum_and_spread.1), calls=%async_computation.1 | async-start | bytes 196608 | tf_op jit(solution)/shard_map/all_to_all | solution.py:530
  32.1 51.1 %copy-start = (bf16[1024,2048]{1,0:T(8,128)(2,1)S(1)}, bf16[1024,2048]{1,0:T(8,128)(2,1)}, u32[]{:S(2)}) copy-start(bf16[1024,2048]{1,0:T(8,128)(2,1)} %w_out.1) | copy-start | bytes 12582916
  32.1 51.1 %copy-start.1 = (bf16[1,192,2048]{2,1,0:T(8,128)(2,1)S(1)}, bf16[1,192,2048]{2,1,0:T(8,128)(2,1)}, u32[]{:S(2)}) copy-start(bf16[1,192,2048]{2,1,0:T(8,128)(2,1)} %latent_in.1) | copy-start | bytes 2359300
  32.1 51.1 %copy-start.2 = (bf16[128]{0:T(256)(128)(2,1)S(1)}, bf16[128]{0:T(256)(128)(2,1)}, u32[]{:S(2)}) copy-start(bf16[128]{0:T(256)(128)(2,1)} %param.32) | copy-start | bytes 772

commit v4 on v3

--- a/solution.py
+++ b/solution.py
@@ -22,6 +22,8 @@
 ROW_OF_X = 4 * SPAN
 
 K_AT, V_AT, Q_AT, S_AT, X_ROWS = 0, 208, 416, 608, 624
+
+FLOPS = 10**10
 
 F32 = jnp.float32
 BF16 = jnp.bfloat16
@@ -79,54 +81,18 @@
         out[k] = value
 
 
-def prepare(
-    gain_in, decay_in, beta_in, rate_in, bias_in, extra_in, latent_in, context_in,
-    w_key_in, w_value_in, w_key, w_value, latent, context, factors, gain, w_small, consts,
-    w_decay, w_beta, rate, bias, extra, sems,
+def project(
+    parts, gain, latent, context, w_key, w_value, w_query, w_gate,
+    decay_in, beta_in, rate_in, bias_in, extra_in,
+    out, gate_out, mods, rows_in, w_decay, w_beta, rate_at, bias_at, extra, sems,
 ):
     copies = fetch(
         (
-            (latent_in, latent), (context_in, context), (gain_in, gain), (decay_in, w_decay),
-            (beta_in, w_beta), (rate_in, rate), (bias_in, bias), (extra_in, extra),
-            (w_key_in, w_key), (w_value_in, w_value),
+            (decay_in, w_decay), (beta_in, w_beta), (rate_in, rate_at), (bias_in, bias_at),
+            (extra_in, extra),
         ),
         sems,
     )
-    for copy in copies[:8]:
-        copy.wait()
-
-    def factor(values):
-        values = values.astype(F32)
-        mean = jnp.mean(values * values, axis=-1, keepdims=True)
-        return jnp.broadcast_to(lax.rsqrt(mean + NORM_EPS), (values.shape[0], LANES))
-
-    for g in range(0, SPAN, 64):
-        factors[g : g + 64, :] = factor(latent[0, g : g + 64, :])
-    factors[SPAN : SPAN + CTX_OWN, :] = factor(context[0])
-    factors[SPAN + CTX_OWN :, :] = jnp.zeros((ROWS - SPAN - CTX_OWN, LANES), F32)
-    w_small[...] = jnp.concatenate(
-        [w[d].astype(F32) for w in (w_decay, w_beta) for d in range(2)], axis=0
-    ).astype(BF16)
-
-    def spread(at):
-        row = iota((4, 256), 0)
-        value = jnp.where(row == 0, at[0, 0], at[0, 1])
-        return jnp.where(row < 2, value, jnp.where(row == 2, at[1, 0], at[1, 1]))
-
-    latent_only = jnp.concatenate([extra[0, 0], extra[0, 1]], axis=0)
-    added = jnp.concatenate([latent_only, jnp.zeros((4, 256 - SPAN), F32)], axis=1)
-    consts[...] = jnp.concatenate(
-        [added, spread(rate), spread(bias), jnp.zeros((4, 256), F32)], axis=0
-    )
-    for copy in copies[8:]:
-        copy.wait()
-
-
-def project(
-    parts, w_key, w_value, latent, context, factors, gain, w_small, consts, w_query_in, w_gate_in,
-    out, gate_out, mods, rows_in, w_query, w_gate, sems,
-):
-    copies = fetch(((w_query_in, w_query), (w_gate_in, w_gate)), sems)
     for y in range(4):
         total = parts[y].astype(F32)
         for x in range(1, 4):
@@ -139,24 +105,46 @@
 
     for j in range(16):
         gate_out[j : j + 1, :] = row(0, 32 + j)
-    none = jnp.zeros((ROWS - SPAN - CTX_OWN, LANES), F32)
-    for which, rows in ((0, slice(0, SPAN)), (1, slice(SPAN, ROWS))):
+
+    def modulate(values, which, at):
+        factor = lax.rsqrt(jnp.mean(values * values, axis=-1, keepdims=True) + NORM_EPS)
         for j in range(16):
             cols = slice(j * LANES, (j + 1) * LANES)
-            if which == 0:
-                values = latent[0, :, cols].astype(F32)
-            else:
-                values = jnp.concatenate([context[0, :, cols].astype(F32), none], axis=0)
             scale = gain[j : j + 1, :].astype(F32) * (1.0 + row(which, 16 + j))
-            tile = values * factors[rows, :] * scale + row(which, j)
-            rows_in[rows, cols] = tile.astype(BF16)
+            tile = values[:, cols] * factor * scale + row(which, j)
+            rows_in[at : at + values.shape[0], cols] = tile.astype(BF16)
+
+    for g in range(0, SPAN, 64):
+        modulate(latent[0, g : g + 64, :].astype(F32), 0, g)
+    none = jnp.zeros((ROWS - SPAN - CTX_OWN, D), F32)
+    modulate(jnp.concatenate([context[0].astype(F32), none], axis=0), 1, SPAN)
     inputs = rows_in[...]
 
     def heads(values):
         return [values[:, h * HEAD : (h + 1) * HEAD] for h in range(2)]
 
-    added, rate, bias = (consts[n : n + 4, :ROWS] for n in (0, 4, 8))
-    small = rounded(dot(w_small[...], inputs, ((1,), (1,))))
+    def unit(v):
+        return v * lax.rsqrt(jnp.sum(v * v, axis=-1, keepdims=True) + NORM_EPS)
+
+    keys = heads(silu(rounded(dot(inputs, w_key[...]))))
+    values = heads(silu(rounded(dot(inputs, w_value[...]))))
+    queries = heads(silu(rounded(dot(inputs[:SPAN], w_query[...]))))
+    gates = heads(silu(rounded(dot(inputs[:SPAN], w_gate[...]))))
+    for copy in copies:
+        copy.wait()
+
+    def column(at):
+        row = iota((4, 1), 0)
+        value = jnp.where(row == 0, at[0, 0], at[0, 1])
+        return jnp.where(row < 2, value, jnp.where(row == 2, at[1, 0], at[1, 1]))
+
+    rate, bias = column(rate_at), column(bias_at)
+    w_small = jnp.concatenate(
+        [w[d].astype(F32) for w in (w_decay, w_beta) for d in range(2)], axis=0
+    ).astype(BF16)
+    latent_only = jnp.concatenate([extra[0, 0], extra[0, 1]], axis=0)
+    added = jnp.concatenate([latent_only, jnp.zeros((4, ROWS - SPAN), F32)], axis=1)
+    small = rounded(dot(w_small, inputs, ((1,), (1,))))
     decay_raw, beta_raw = small[:4], small[4:]
     pre = decay_raw + bias
     soft = jnp.maximum(pre, 0.0) + jnp.log1p(jnp.exp(-jnp.abs(pre)))
@@ -166,15 +154,6 @@
     g_high, g_low = split_in_two(jnp.concatenate([log_decay, pad], axis=1))
     b_high, b_low = split_in_two(jnp.concatenate([beta, pad], axis=1))
 
-    def unit(v):
-        return v * lax.rsqrt(jnp.sum(v * v, axis=-1, keepdims=True) + NORM_EPS)
-
-    keys = heads(silu(rounded(dot(inputs, w_key[...]))))
-    values = heads(silu(rounded(dot(inputs, w_value[...]))))
-    copies[0].wait()
-    queries = heads(silu(rounded(dot(inputs[:SPAN], w_query[...]))))
-    copies[1].wait()
-    gates = heads(silu(rounded(dot(inputs[:SPAN], w_gate[...]))))
     low_lanes = iota((ROWS, LANES), 1) < 64
     for h in range(2):
         key = unit(keys[h]).astype(BF16)
@@ -272,19 +251,27 @@
     def block(self, key, rows):
         n = key.shape[0]
         pairs = dot(key, key, ((1,), (1,)))
-        rates = dot(self.same, rows, ((1,), (1,)))
+        rows32 = rows.astype(F32)
         key32 = key.astype(F32)
+
+        def down_columns(matrix, at):
+            two = [jnp.broadcast_to(rows32[r : r + 1], (LANES, n)) for r in (at, at + 1)]
+            both = dot(matrix, jnp.concatenate(two, axis=0).astype(BF16), ((1,), (1,)))
+            return both[:, :LANES] + both[:, LANES:]
+
+        wide = lambda v: jnp.concatenate([v] * (n // LANES), axis=1)
         found = []
         for d in range(2):
-            sums = dot(self.upto[d], rows, ((1,), (1,)))
-            down = sums[:, 4 * d : 4 * d + 1] + sums[:, 4 * d + 1 : 4 * d + 2]
-            across = dot(rows, self.upto[d], ((1,), (1,)))
+            down = down_columns(self.upto[d], 4 * d)
+            beta = down_columns(self.same, 4 * d + 2)
+            across = dot(rows, self.upto[1 - d])
             along = across[4 * d : 4 * d + 1] + across[4 * d + 1 : 4 * d + 2]
             reach = self.away if d == 0 else -self.away
-            weights = jnp.where(reach >= 0, jnp.exp(jnp.where(reach >= 0, down - along, 0.0)), 0.0)
-            beta = rates[:, 4 * d + 2 : 4 * d + 3] + rates[:, 4 * d + 3 : 4 * d + 4]
+            weights = jnp.where(
+                reach >= 0, jnp.exp(jnp.where(reach >= 0, wide(down) - along, 0.0)), 0.0
+            )
             total = down[n - 1 : n] if d == 0 else down[0:1]
-            low = jnp.where(reach > 0, pairs * weights * beta, 0.0)
+            low = jnp.where(reach > 0, pairs * weights * wide(beta), 0.0)
             kept = (key32 * jnp.exp(total - down)).astype(BF16)
             found.append((low, beta, jnp.exp(down), kept, jnp.exp(total), weights))
         return found
@@ -505,7 +492,7 @@
 HBM = pl.BlockSpec(memory_space=pltpu.HBM)
 
 
-def call(body, name, n_in, outs, scratch=(), mib=16, n_hbm=0):
+def call(body, name, n_in, outs, scratch=(), mib=16, n_hbm=0, flops=None):
     many = isinstance(outs, (list, tuple))
     return pl.pallas_call(
         body,
@@ -513,6 +500,7 @@
         in_specs=[VM] * n_in + [HBM] * n_hbm,
         out_specs=[VM] * len(outs) if many else VM,
         scratch_shapes=list(scratch),
+        cost_estimate=flops and pl.CostEstimate(flops, 0, 0),
         compiler_params=pltpu.CompilerParams(vmem_limit_bytes=mib << 20),
         name=name,
     )
@@ -534,23 +522,6 @@
     latent, cond, context, ctx_cond, w_mod, norm_gain, w_query, w_key, w_value, w_outgate,
     w_decay, w_beta, decay_rate, decay_bias, extra_decay, out_gain, w_out,
 ):
-    by_row = lambda w: w.transpose(1, 2, 0)
-    fetched = (
-        norm_gain.reshape(16, LANES), by_row(w_decay), by_row(w_beta), decay_rate, decay_bias,
-        extra_decay, latent, context, w_key, w_value,
-    )
-    space = lambda n: pltpu.SMEM if n in (3, 4) else pltpu.VMEM
-    prepared = call(
-        prepare, "prepare", 0,
-        [shape(w.shape) for w in fetched[8:]]
-        + [
-            shape(latent.shape), shape(context.shape), shape((ROWS, LANES), F32),
-            shape((16, LANES)), shape((8, D)), shape((16, 256), F32),
-        ],
-        [space(n)(a.shape, a.dtype) for n, a in enumerate(fetched) if 1 <= n <= 5]
-        + [pltpu.SemaphoreType.DMA((len(fetched),))],
-        16, len(fetched),
-    )(*(in_hbm(a) for a in fetched))
     partial = call(
         partial_modulation, "partial_modulation", 0, shape((8, 24, LANES)),
         [
@@ -558,16 +529,25 @@
             pltpu.VMEM(cond.shape, BF16), pltpu.VMEM(w_mod.shape, BF16),
             pltpu.SemaphoreType.DMA((3,)),
         ],
-        16, 3,
+        16, 3, FLOPS,
     )(in_hbm(cond), in_hbm(ctx_cond[None, :]), in_hbm(w_mod))
-    summed = call(sum_and_spread, "sum_and_spread", 1, shape((16, 24, LANES)))(swap(partial, "z"))
+    summed = call(
+        sum_and_spread, "sum_and_spread", 1, shape((16, 24, LANES)), flops=FLOPS
+    )(swap(partial, "z"))
     parts = swap(summed, ("x", "tp"))
+    by_row = lambda w: w.transpose(1, 2, 0)
+    fetched = (by_row(w_decay), by_row(w_beta), decay_rate, decay_bias, extra_decay)
+    space = lambda n: pltpu.SMEM if n in (2, 3) else pltpu.VMEM
     sent, gate = call(
-        project, "project", 1 + len(prepared), [shape((4, X_ROWS, LANES)), shape((16, LANES), F32)],
+        project, "project", 8, [shape((4, X_ROWS, LANES)), shape((16, LANES), F32)],
         [pltpu.VMEM((96, LANES), F32), pltpu.VMEM((ROWS, D), BF16)]
-        + [pltpu.VMEM(w_query.shape, BF16)] * 2 + [pltpu.SemaphoreType.DMA((2,))],
-        24, 2,
-    )(parts, *prepared, in_hbm(w_query), in_hbm(w_outgate))
+        + [space(n)(a.shape, a.dtype) for n, a in enumerate(fetched)]
+        + [pltpu.SemaphoreType.DMA((len(fetched),))],
+        16, len(fetched),
+    )(
+        parts, norm_gain.reshape(16, LANES), latent, context, w_key, w_value, w_query, w_outgate,
+        *(in_hbm(a) for a in fetched),
+    )
     held = swap(sent, "x")
     maps, reads, offsets = call(
         token_maps, "token_maps", 1,

time: 85.3 us -> 83.3 us (0.977)
  blocking collectives: 55 us -> 68.8 us
  starting transfers between devices: 7.48 us -> 0 us
  waiting for transfers between devices: 4.36 us -> 0 us
  Pallas kernels: 18.1 us -> 14 us
    all_to_all x4 -> x5, blocking collectives: 55 us -> 68.8 us  [swap(): return lax.all_to_all(array, axes, 0, 0, tiled=True)]
    all_to_all x1 -> x0, starting transfers between devices: 7.48 us -> none  [swap(): return lax.all_to_all(array, axes, 0, 0, tiled=True)]
    all_to_all x1 -> x0, waiting for transfers between devices: 4.36 us -> none  [swap(): return lax.all_to_all(array, axes, 0, 0, tiled=True)]
    pallas_call x3 -> x2, Pallas kernels: 6.57 us -> 2.8 us  [the longest x1 2.78 us: on_device(): call(project, 'project', 8, [shape((4, X_ROWS, LANES)), shape((16, LANES)...]
  transfers between devices with their start and end apart: 1 -> 0, of which waited for: 1 -> 0; matrix products, arithmetic and copies ran while one was open for 0% -> 0% of each run, Pallas kernels for 2% -> 0%
where the time goes in v4:
time: 83.3 us; the launch traced here: 83 us
  blocking collectives  68.8 us (83%)
  Pallas kernels  14 us (17%)
    all_to_all x5, blocking collectives, swap(): return lax.all_to_all(array, axes, 0, 0, tiled=True)  68.8 us
    pallas_call x1, Pallas kernels, on_device(): call(token_maps, 'token_maps', 1, [shape((8, HEAD, 256)), shape((ROW_OF_X...  5.11 us
    pallas_call x1, Pallas kernels, on_device(): call(read_states, 'read_states', 4, shape((16, 48, LANES)))  3.21 us
    pallas_call x1, Pallas kernels, on_device(): call(project, 'project', 8, [shape((4, X_ROWS, LANES)), shape((16, LANES)...  2.78 us
    pallas_call x1, Pallas kernels, on_device(): call(mix, 'mix', 5, shape((48, D)))  1.78 us

profile of v4, /device:TPU:2, one launch (start us, length us, event | category | flops | bytes accessed | tf_op | source)
XLA Modules:
  0.0 83.0 jit_solution(8986679649169823643)
XLA Ops:
  0.0 1.1 %partial_modulation.1 = bf16[8,24,128]{2,1,0:T(8,128)(2,1)S(1)} custom-call(bf16[1,64]{1,0:T(2,128)(2,1)} %cond_in.1, bf16[1,64]{1,0:T(2,128)(2,1)} %bitcast.12, bf16[64,1536]{1,0:T(8,128)(2,1)} %w_mod_in.1), custom_call_target="tpu_custom_call" | custom-call | flops 10000000000 | tf_op jit(solution)/shard_map/partial_modulation/pallas_call | solution.py:525
  1.1 16.5 %all_to_all.25.parts = bf16[8,24,128]{2,1,0:T(8,128)(2,1)S(1)} all-to-all(bf16[8,24,128]{2,1,0:T(8,128)(2,1)S(1)} %partial_modulation.1), channel_id=1, replica_groups=mesh['z'=8,'x'=4,'tp'=4,'dp'=2] {'z'}, dimensions={0} | all-to-all | bytes 98304 | tf_op jit(solution)/shard_map/all_to_all | solution.py:518
  17.6 0.0 copy-start.1
  17.6 0.0 copy-start.2
  17.6 0.0 copy-start.3
  17.6 0.0 copy-start.4
  17.6 0.0 copy-start.5
  17.6 0.0 copy-start.6
  17.6 0.0 copy-start.7
  17.7 13.9 %all_to_all.26.parts = bf16[16,24,128]{2,1,0:T(8,128)(2,1)S(1)} all-to-all(bf16[16,24,128]{2,1,0:T(8,128)(2,1)S(1)} %sum_and_spread.1), channel_id=1, replica_groups=mesh['z'=8,'x'=4,'tp'=4,'dp'=2] {'x','tp'}, dimensions={0} | all-to-all | bytes 196608 | tf_op jit(solution)/shard_map/all_to_all | solution.py:518
  31.5 0.0 copy-done.1
  31.5 0.0 copy-done.2
  31.5 0.0 copy-done.3
  31.5 0.0 copy-done.4
  31.5 0.0 copy-done.5
  31.6 0.0 copy-done.6
  31.6 0.0 copy-done.7
  31.6 0.0 copy-start
  31.6 0.0 copy-start.8
  31.6 2.8 %project.1 = (bf16[4,624,128]{2,1,0:T(8,128)(2,1)S(1)}, f32[16,128]{1,0:T(8,128)S(1)}) custom-call(bf16[16,24,128]{2,1,0:T(8,128)(2,1)S(1)} %all_to_all.26.parts, bf16[16,128]{1,0:T(8,128)(2,1)S(1)} %bitcast.8, bf16[1,192,2048]{2,1,0:T(8,128)(2,1)S(1)} %copy-done.1, bf16[1,8,2048]{2,1,0:T(8,128)(2,1)S(1)} %copy-done.6, bf16[2048,256]{1,0:T(8,128)(2,1)S(1)} %copy-done.2, ...), custom_call_target="tpu_custom_call" | custom-call | tf_op jit(solution)/shard_map/project/pallas_call | solution.py:541
  34.4 11.2 %all_to_all.27.got.sent = bf16[4,624,128]{2,1,0:T(8,128)(2,1)S(1)} all-to-all(bf16[4,624,128]{2,1,0:T(8,128)(2,1)S(1)} %get-tuple-element.10), channel_id=1, replica_groups=mesh['z'=8,'x'=4,'tp'=4,'dp'=2] {'x'}, dimensions={0} | all-to-all | bytes 1277952 | tf_op jit(solution)/shard_map/all_to_all | solution.py:518
  45.6 5.1 %token_maps.1 = (bf16[8,128,256]{2,1,0:T(8,128)(2,1)S(1)}, bf16[768,256]{1,0:T(8,128)(2,1)S(1)}, f32[768,128]{1,0:T(8,128)S(1)}) custom-call(bf16[4,624,128]{2,1,0:T(8,128)(2,1)S(1)} %all_to_all.27.got.sent), custom_call_target="tpu_custom_call" | custom-call | tf_op jit(solution)/shard_map/token_maps/pallas_call | solution.py:552
  50.7 16.2 %all_to_all.28.got = bf16[8,128,256]{2,1,0:T(8,128)(2,1)S(1)} all-to-all(bf16[8,128,256]{2,1,0:T(8,128)(2,1)S(1)} %get-tuple-element.11), channel_id=1, replica_groups=mesh['z'=8,'x'=4,'tp'=4,'dp'=2] {'z'}, dimensions={0} | all-to-all | bytes 1048576 | tf_op jit(solution)/shard_map/all_to_all | solution.py:518
  66.8 3.2 %read_states.1 = bf16[16,48,128]{2,1,0:T(8,128)(2,1)S(1)} custom-call(bf16[8,128,256]{2,1,0:T(8,128)(2,1)S(1)} %all_to_all.28.got, bf16[768,256]{1,0:T(8,128)(2,1)S(1)} %get-tuple-element.12.reads, f32[768,128]{1,0:T(8,128)S(1)} %get-tuple-element.13.offsets, bf16[4,624,128]{2,1,0:T(8,128)(2,1)S(1)} %all_to_all.27.got.sent), custom_call_target="tpu_custom_call" | custom-call | tf_op jit(solution)/shard_map/read_states/pallas_call | solution.py:560
  70.1 11.2 %all_to_all.29.got = bf16[16,48,128]{2,1,0:T(8,128)(2,1)S(1)} all-to-all(bf16[16,48,128]{2,1,0:T(8,128)(2,1)S(1)} %read_states.1), channel_id=1, replica_groups=mesh['z'=8,'x'=4,'tp'=4,'dp'=2] {'x','tp'}, dimensions={0} | all-to-all | bytes 393216 | tf_op jit(solution)/shard_map/all_to_all | solution.py:518
  81.2 0.0 copy-done
  81.2 0.0 copy-done.8
  81.2 1.8 %mix.1 = bf16[48,2048]{1,0:T(8,128)(2,1)} custom-call(bf16[16,48,128]{2,1,0:T(8,128)(2,1)S(1)} %all_to_all.29.got, bf16[1,128]{1,0:T(2,128)(2,1)S(1)} %bitcast.9, f32[16,128]{1,0:T(8,128)S(1)} %get-tuple-element.14.gate, bf16[1024,2048]{1,0:T(8,128)(2,1)S(1)} %copy-done, bf16[192,2048]{1,0:T(8,128)(2,1)S(1)} %bitcast.7), custom_call_target="tpu_custom_call" | custom-call | tf_op jit(solution)/shard_map/mix/pallas_call | solution.py:564
  (1 shorter events, 0.0 us)
Async XLA Ops:
  17.6 13.9 %copy-start.1 = (bf16[1,192,2048]{2,1,0:T(8,128)(2,1)S(1)}, bf16[1,192,2048]{2,1,0:T(8,128)(2,1)}, u32[]{:S(2)}) copy-start(bf16[1,192,2048]{2,1,0:T(8,128)(2,1)} %latent.1) | copy-start | bytes 2359300
  17.6 13.9 %copy-start.2 = (bf16[2048,256]{1,0:T(8,128)(2,1)S(1)}, bf16[2048,256]{1,0:T(8,128)(2,1)}, u32[]{:S(2)}) copy-start(bf16[2048,256]{1,0:T(8,128)(2,1)} %w_key.1) | copy-start | bytes 3145732
  17.6 13.9 %copy-start.3 = (bf16[2048,256]{1,0:T(8,128)(2,1)S(1)}, bf16[2048,256]{1,0:T(8,128)(2,1)}, u32[]{:S(2)}) copy-start(bf16[2048,256]{1,0:T(8,128)(2,1)} %w_value.1) | copy-start | bytes 3145732
  17.6 13.9 %copy-start.4 = (bf16[2048,256]{1,0:T(8,128)(2,1)S(1)}, bf16[2048,256]{1,0:T(8,128)(2,1)}, u32[]{:S(2)}) copy-start(bf16[2048,256]{1,0:T(8,128)(2,1)} %w_query.1) | copy-start | bytes 3145732
  17.6 13.9 %copy-start.5 = (bf16[2048,256]{1,0:T(8,128)(2,1)S(1)}, bf16[2048,256]{1,0:T(8,128)(2,1)}, u32[]{:S(2)}) copy-start(bf16[2048,256]{1,0:T(8,128)(2,1)} %w_gate.1) | copy-start | bytes 3145732
  17.6 13.9 %copy-start.6 = (bf16[1,8,2048]{2,1,0:T(8,128)(2,1)S(1)}, bf16[1,8,2048]{2,1,0:T(8,128)(2,1)}, u32[]{:S(2)}) copy-start(bf16[1,8,2048]{2,1,0:T(8,128)(2,1)} %context.1) | copy-start | bytes 98308
  17.6 13.9 %copy-start.7 = (bf16[2048]{0:T(1024)(128)(2,1)S(1)}, bf16[2048]{0:T(1024)(128)(2,1)}, u32[]{:S(2)}) copy-start(bf16[2048]{0:T(1024)(128)(2,1)} %param.22) | copy-start | bytes 12292
  31.6 49.7 %copy-start = (bf16[1024,2048]{1,0:T(8,128)(2,1)S(1)}, bf16[1024,2048]{1,0:T(8,128)(2,1)}, u32[]{:S(2)}) copy-start(bf16[1024,2048]{1,0:T(8,128)(2,1)} %w_out.1) | copy-start | bytes 12582916
  31.6 49.7 %copy-start.8 = (bf16[128]{0:T(256)(128)(2,1)S(1)}, bf16[128]{0:T(256)(128)(2,1)}, u32[]{:S(2)}) copy-start(bf16[128]{0:T(256)(128)(2,1)} %param.32) | copy-start | bytes 772

commit v5 on v4

--- a/solution.py
+++ b/solution.py
@@ -83,16 +83,8 @@
 
 def project(
     parts, gain, latent, context, w_key, w_value, w_query, w_gate,
-    decay_in, beta_in, rate_in, bias_in, extra_in,
-    out, gate_out, mods, rows_in, w_decay, w_beta, rate_at, bias_at, extra, sems,
+    w_decay, w_beta, rate_at, bias_at, extra, out, gate_out, mods, rows_in,
 ):
-    copies = fetch(
-        (
-            (decay_in, w_decay), (beta_in, w_beta), (rate_in, rate_at), (bias_in, bias_at),
-            (extra_in, extra),
-        ),
-        sems,
-    )
     for y in range(4):
         total = parts[y].astype(F32)
         for x in range(1, 4):
@@ -130,13 +122,11 @@
     values = heads(silu(rounded(dot(inputs, w_value[...]))))
     queries = heads(silu(rounded(dot(inputs[:SPAN], w_query[...]))))
     gates = heads(silu(rounded(dot(inputs[:SPAN], w_gate[...]))))
-    for copy in copies:
-        copy.wait()
-
     def column(at):
         row = iota((4, 1), 0)
-        value = jnp.where(row == 0, at[0, 0], at[0, 1])
-        return jnp.where(row < 2, value, jnp.where(row == 2, at[1, 0], at[1, 1]))
+        one = jnp.where(row == 0, at[0:1, 0:1], at[0:1, 1:2])
+        two = jnp.where(row == 2, at[1:2, 0:1], at[1:2, 1:2])
+        return jnp.where(row < 2, one, two)
 
     rate, bias = column(rate_at), column(bias_at)
     w_small = jnp.concatenate(
@@ -536,17 +526,12 @@
     )(swap(partial, "z"))
     parts = swap(summed, ("x", "tp"))
     by_row = lambda w: w.transpose(1, 2, 0)
-    fetched = (by_row(w_decay), by_row(w_beta), decay_rate, decay_bias, extra_decay)
-    space = lambda n: pltpu.SMEM if n in (2, 3) else pltpu.VMEM
     sent, gate = call(
-        project, "project", 8, [shape((4, X_ROWS, LANES)), shape((16, LANES), F32)],
-        [pltpu.VMEM((96, LANES), F32), pltpu.VMEM((ROWS, D), BF16)]
-        + [space(n)(a.shape, a.dtype) for n, a in enumerate(fetched)]
-        + [pltpu.SemaphoreType.DMA((len(fetched),))],
-        16, len(fetched),
+        project, "project", 13, [shape((4, X_ROWS, LANES)), shape((16, LANES), F32)],
+        [pltpu.VMEM((96, LANES), F32), pltpu.VMEM((ROWS, D), BF16)],
     )(
         parts, norm_gain.reshape(16, LANES), latent, context, w_key, w_value, w_query, w_outgate,
-        *(in_hbm(a) for a in fetched),
+        by_row(w_decay), by_row(w_beta), decay_rate, decay_bias, extra_decay,
     )
     held = swap(sent, "x")
     maps, reads, offsets = call(

time: 83.3 us -> 82.3 us (0.988)
  Pallas kernels: 14 us -> 12.9 us
    pallas_call x1, Pallas kernels: 2.78 us -> 1.66 us  [on_device(): call(project, 'project', 13, [shape((4, X_ROWS, LANES)), shape((16, LANES...]
where the time goes in v5:
time: 82.3 us; the launch traced here: 82 us
  blocking collectives  68.8 us (84%)
  Pallas kernels  12.9 us (16%)
    all_to_all x5, blocking collectives, swap(): return lax.all_to_all(array, axes, 0, 0, tiled=True)  68.8 us
    pallas_call x1, Pallas kernels, on_device(): call(token_maps, 'token_maps', 1, [shape((8, HEAD, 256)), shape((ROW_OF_X...  5.11 us
    pallas_call x1, Pallas kernels, on_device(): call(read_states, 'read_states', 4, shape((16, 48, LANES)))  3.21 us
    pallas_call x1, Pallas kernels, on_device(): call(mix, 'mix', 5, shape((48, D)))  1.77 us
    pallas_call x1, Pallas kernels, on_device(): call(project, 'project', 13, [shape((4, X_ROWS, LANES)), shape((16, LANES...  1.66 us

profile of v5, /device:TPU:2, one launch (start us, length us, event | category | flops | bytes accessed | tf_op | source)
XLA Modules:
  0.0 82.0 jit_solution(14371747465397671747)
XLA Ops:
  0.0 1.1 %partial_modulation.1 = bf16[8,24,128]{2,1,0:T(8,128)(2,1)S(1)} custom-call(bf16[1,64]{1,0:T(2,128)(2,1)} %cond_in.1, bf16[1,64]{1,0:T(2,128)(2,1)} %bitcast.12, bf16[64,1536]{1,0:T(8,128)(2,1)} %w_mod_in.1), custom_call_target="tpu_custom_call" | custom-call | flops 10000000000 | tf_op jit(solution)/shard_map/partial_modulation/pallas_call | solution.py:515
  1.1 16.5 %all_to_all.25.parts = bf16[8,24,128]{2,1,0:T(8,128)(2,1)S(1)} all-to-all(bf16[8,24,128]{2,1,0:T(8,128)(2,1)S(1)} %partial_modulation.1), channel_id=1, replica_groups=mesh['z'=8,'x'=4,'tp'=4,'dp'=2] {'z'}, dimensions={0} | all-to-all | bytes 98304 | tf_op jit(solution)/shard_map/all_to_all | solution.py:508
  17.6 0.0 copy-start.5
  17.6 0.0 copy-start.6
  17.6 0.0 copy-start.7
  17.6 0.0 copy-start.8
  17.7 0.0 copy-start.9
  17.7 0.0 copy-start.10
  17.7 0.0 copy-start.11
  17.7 0.0 copy-start.12
  17.7 13.9 %all_to_all.26.parts = bf16[16,24,128]{2,1,0:T(8,128)(2,1)S(1)} all-to-all(bf16[16,24,128]{2,1,0:T(8,128)(2,1)S(1)} %sum_and_spread.1), channel_id=1, replica_groups=mesh['z'=8,'x'=4,'tp'=4,'dp'=2] {'x','tp'}, dimensions={0} | all-to-all | bytes 196608 | tf_op jit(solution)/shard_map/all_to_all | solution.py:508
  31.6 0.0 copy-done.1
  31.6 0.0 copy-done.2
  31.6 0.0 copy-done.3
  31.6 0.0 copy-done.4
  31.6 0.0 copy-done.5
  31.6 0.0 copy-done.6
  31.6 0.0 copy-done.7
  31.6 0.0 copy-done.8
  31.6 0.0 copy-done.9
  31.7 0.0 copy-done.10
  31.7 0.0 copy-done.11
  31.7 0.0 copy-done.12
  31.7 0.0 copy-start
  31.7 0.0 copy-start.13
  31.7 1.7 %project.1 = (bf16[4,624,128]{2,1,0:T(8,128)(2,1)S(1)}, f32[16,128]{1,0:T(8,128)S(1)}) custom-call(bf16[16,24,128]{2,1,0:T(8,128)(2,1)S(1)} %all_to_all.26.parts, bf16[16,128]{1,0:T(8,128)(2,1)S(1)} %bitcast.10, bf16[1,192,2048]{2,1,0:T(8,128)(2,1)S(1)} %copy-done.1, bf16[1,8,2048]{2,1,0:T(8,128)(2,1)S(1)} %copy-done.6, bf16[2048,256]{1,0:T(8,128)(2,1)S(1)} %copy-done.2, ...), custom_call_target="tpu_custom_call" | custom-call | tf_op jit(solution)/shard_map/project/pallas_call | solution.py:529
  33.4 11.2 %all_to_all.27.got.sent = bf16[4,624,128]{2,1,0:T(8,128)(2,1)S(1)} all-to-all(bf16[4,624,128]{2,1,0:T(8,128)(2,1)S(1)} %get-tuple-element.10), channel_id=1, replica_groups=mesh['z'=8,'x'=4,'tp'=4,'dp'=2] {'x'}, dimensions={0} | all-to-all | bytes 1277952 | tf_op jit(solution)/shard_map/all_to_all | solution.py:508
  44.5 5.1 %token_maps.1 = (bf16[8,128,256]{2,1,0:T(8,128)(2,1)S(1)}, bf16[768,256]{1,0:T(8,128)(2,1)S(1)}, f32[768,128]{1,0:T(8,128)S(1)}) custom-call(bf16[4,624,128]{2,1,0:T(8,128)(2,1)S(1)} %all_to_all.27.got.sent), custom_call_target="tpu_custom_call" | custom-call | tf_op jit(solution)/shard_map/token_maps/pallas_call | solution.py:537
  49.7 16.2 %all_to_all.28.got = bf16[8,128,256]{2,1,0:T(8,128)(2,1)S(1)} all-to-all(bf16[8,128,256]{2,1,0:T(8,128)(2,1)S(1)} %get-tuple-element.11), channel_id=1, replica_groups=mesh['z'=8,'x'=4,'tp'=4,'dp'=2] {'z'}, dimensions={0} | all-to-all | bytes 1048576 | tf_op jit(solution)/shard_map/all_to_all | solution.py:508
  65.8 3.2 %read_states.1 = bf16[16,48,128]{2,1,0:T(8,128)(2,1)S(1)} custom-call(bf16[8,128,256]{2,1,0:T(8,128)(2,1)S(1)} %all_to_all.28.got, bf16[768,256]{1,0:T(8,128)(2,1)S(1)} %get-tuple-element.12.reads, f32[768,128]{1,0:T(8,128)S(1)} %get-tuple-element.13.offsets, bf16[4,624,128]{2,1,0:T(8,128)(2,1)S(1)} %all_to_all.27.got.sent), custom_call_target="tpu_custom_call" | custom-call | tf_op jit(solution)/shard_map/read_states/pallas_call | solution.py:545
  69.1 11.2 %all_to_all.29.got = bf16[16,48,128]{2,1,0:T(8,128)(2,1)S(1)} all-to-all(bf16[16,48,128]{2,1,0:T(8,128)(2,1)S(1)} %read_states.1), channel_id=1, replica_groups=mesh['z'=8,'x'=4,'tp'=4,'dp'=2] {'x','tp'}, dimensions={0} | all-to-all | bytes 393216 | tf_op jit(solution)/shard_map/all_to_all | solution.py:508
  80.2 1.8 %mix.1 = bf16[48,2048]{1,0:T(8,128)(2,1)} custom-call(bf16[16,48,128]{2,1,0:T(8,128)(2,1)S(1)} %all_to_all.29.got, bf16[1,128]{1,0:T(2,128)(2,1)S(1)} %bitcast.11, f32[16,128]{1,0:T(8,128)S(1)} %get-tuple-element.14.gate, bf16[1024,2048]{1,0:T(8,128)(2,1)S(1)} %copy-done, bf16[192,2048]{1,0:T(8,128)(2,1)S(1)} %bitcast.7), custom_call_target="tpu_custom_call" | custom-call | tf_op jit(solution)/shard_map/mix/pallas_call | solution.py:549
  (7 shorter events, 0.0 us)
Async XLA Ops:
  17.6 14.0 %copy-start.1 = (bf16[1,192,2048]{2,1,0:T(8,128)(2,1)S(1)}, bf16[1,192,2048]{2,1,0:T(8,128)(2,1)}, u32[]{:S(2)}) copy-start(bf16[1,192,2048]{2,1,0:T(8,128)(2,1)} %latent.1) | copy-start | bytes 2359300
  17.6 14.0 %copy-start.2 = (bf16[2048,256]{1,0:T(8,128)(2,1)S(1)}, bf16[2048,256]{1,0:T(8,128)(2,1)}, u32[]{:S(2)}) copy-start(bf16[2048,256]{1,0:T(8,128)(2,1)} %w_key.1) | copy-start | bytes 3145732
  17.6 14.0 %copy-start.3 = (bf16[2048,256]{1,0:T(8,128)(2,1)S(1)}, bf16[2048,256]{1,0:T(8,128)(2,1)}, u32[]{:S(2)}) copy-start(bf16[2048,256]{1,0:T(8,128)(2,1)} %w_value.1) | copy-start | bytes 3145732
  17.6 14.0 %copy-start.4 = (bf16[2048,256]{1,0:T(8,128)(2,1)S(1)}, bf16[2048,256]{1,0:T(8,128)(2,1)}, u32[]{:S(2)}) copy-start(bf16[2048,256]{1,0:T(8,128)(2,1)} %w_query.1) | copy-start | bytes 3145732
  17.6 14.0 %copy-start.5 = (bf16[2048,256]{1,0:T(8,128)(2,1)S(1)}, bf16[2048,256]{1,0:T(8,128)(2,1)}, u32[]{:S(2)}) copy-start(bf16[2048,256]{1,0:T(8,128)(2,1)} %w_gate.1) | copy-start | bytes 3145732
  17.6 14.0 %copy-start.6 = (bf16[1,8,2048]{2,1,0:T(8,128)(2,1)S(1)}, bf16[1,8,2048]{2,1,0:T(8,128)(2,1)}, u32[]{:S(2)}) copy-start(bf16[1,8,2048]{2,1,0:T(8,128)(2,1)} %context.1) | copy-start | bytes 98308
  17.6 14.0 %copy-start.7 = (bf16[2048,2,2]{0,2,1:T(2,128)(2,1)S(1)}, bf16[2048,2,2]{0,2,1:T(2,128)(2,1)}, u32[]{:S(2)}) copy-start(bf16[2048,2,2]{0,2,1:T(2,128)(2,1)} %param.27) | copy-start | bytes 49156
  17.6 14.0 %copy-start.8 = (bf16[2048,2,2]{0,2,1:T(2,128)(2,1)S(1)}, bf16[2048,2,2]{0,2,1:T(2,128)(2,1)}, u32[]{:S(2)}) copy-start(bf16[2048,2,2]{0,2,1:T(2,128)(2,1)} %param.28) | copy-start | bytes 49156
  17.7 14.0 %copy-start.9 = (bf16[2048]{0:T(1024)(128)(2,1)S(1)}, bf16[2048]{0:T(1024)(128)(2,1)}, u32[]{:S(2)}) copy-start(bf16[2048]{0:T(1024)(128)(2,1)} %param.22) | copy-start | bytes 12292
  17.7 14.0 %copy-start.10 = (f32[1,2,2,192]{3,2,1,0:T(2,128)S(1)}, f32[1,2,2,192]{3,2,1,0:T(2,128)}, u32[]{:S(2)}) copy-start(f32[1,2,2,192]{3,2,1,0:T(2,128)} %extra.1) | copy-start | bytes 9220
  17.7 14.0 %copy-start.11 = (f32[2,2]{1,0:T(2,128)S(1)}, f32[2,2]{1,0:T(2,128)}, u32[]{:S(2)}) copy-start(f32[2,2]{1,0:T(2,128)} %rate_at.1) | copy-start | bytes 52
  17.7 14.0 %copy-start.12 = (f32[2,2]{1,0:T(2,128)S(1)}, f32[2,2]{1,0:T(2,128)}, u32[]{:S(2)}) copy-start(f32[2,2]{1,0:T(2,128)} %bias_at.1) | copy-start | bytes 52
  31.7 48.6 %copy-start = (bf16[1024,2048]{1,0:T(8,128)(2,1)S(1)}, bf16[1024,2048]{1,0:T(8,128)(2,1)}, u32[]{:S(2)}) copy-start(bf16[1024,2048]{1,0:T(8,128)(2,1)} %w_out.1) | copy-start | bytes 12582916
  31.7 48.5 %copy-start.13 = (bf16[128]{0:T(256)(128)(2,1)S(1)}, bf16[128]{0:T(256)(128)(2,1)}, u32[]{:S(2)}) copy-start(bf16[128]{0:T(256)(128)(2,1)} %param.32) | copy-start | bytes 772

commit v6 on v5

--- a/solution.py
+++ b/solution.py
@@ -453,7 +453,7 @@
             out[4 * x + y] = jnp.where(left, o[own], gates[own]).astype(BF16)
 
 
-def mix(got, out_gain, gate, w_out, latent, out):
+def mix(got, out_gain, gate, w_out, latent, out_at, out, sems):
     left = iota((48, LANES), 1) < 64
     gain = out_gain[...].astype(F32)
     tiles = []
@@ -468,12 +468,18 @@
     gated = jnp.concatenate(tiles, axis=1)
     start = pl.multiple_of(lax.axis_index("tp") * 48, 16)
     own = latent[pl.ds(start, 48), :].astype(F32)
+    copies = []
     for n in range(0, D, 512):
         mixed = dot(gated, w_out[:, n : n + 512])
         for c in range(0, 512, LANES):
             j = (n + c) // LANES
             cols = slice(n + c, n + c + LANES)
             out[:, cols] = (own[:, cols] + gate[j : j + 1, :] * mixed[:, c : c + LANES]).astype(BF16)
+        part = (slice(None), pl.ds(n, 512))
+        copies.append(pltpu.make_async_copy(out.at[part], out_at.at[part], sems.at[n // 512]))
+        copies[-1].start()
+    for copy in copies:
+        copy.wait()
 
 
 VM = pl.BlockSpec(memory_space=pltpu.VMEM)
@@ -482,13 +488,13 @@
 HBM = pl.BlockSpec(memory_space=pltpu.HBM)
 
 
-def call(body, name, n_in, outs, scratch=(), mib=16, n_hbm=0, flops=None):
+def call(body, name, n_in, outs, scratch=(), mib=16, n_hbm=0, flops=None, out_space=VM):
     many = isinstance(outs, (list, tuple))
     return pl.pallas_call(
         body,
         out_shape=outs,
         in_specs=[VM] * n_in + [HBM] * n_hbm,
-        out_specs=[VM] * len(outs) if many else VM,
+        out_specs=[VM] * len(outs) if many else out_space,
         scratch_shapes=list(scratch),
         cost_estimate=flops and pl.CostEstimate(flops, 0, 0),
         compiler_params=pltpu.CompilerParams(vmem_limit_bytes=mib << 20),
@@ -546,7 +552,10 @@
         reached, reads, offsets, held
     )
     gathered = swap(outs, ("x", "tp"))
-    mixed = call(mix, "mix", 5, shape((48, D)))(
+    mixed = call(
+        mix, "mix", 5, shape((48, D)),
+        [pltpu.VMEM((48, D), BF16), pltpu.SemaphoreType.DMA((4,))], out_space=HBM,
+    )(
         gathered, out_gain[None, :], gate, w_out, latent[0]
     )
     return mixed[None]

time: 82.3 us -> 82.2 us (level)
  no operation moved by 1% of the time
where the time goes in v6:
time: 82.2 us; the launch traced here: 82 us
  blocking collectives  68.8 us (84%)
  Pallas kernels  12.9 us (16%)
    all_to_all x5, blocking collectives, swap(): return lax.all_to_all(array, axes, 0, 0, tiled=True)  68.8 us
    pallas_call x1, Pallas kernels, on_device(): call(token_maps, 'token_maps', 1, [shape((8, HEAD, 256)), shape((ROW_OF_X...  5.11 us
    pallas_call x1, Pallas kernels, on_device(): call(read_states, 'read_states', 4, shape((16, 48, LANES)))  3.21 us
    pallas_call x1, Pallas kernels, on_device(): call(mix, 'mix', 5, shape((48, D)), [pltpu.VMEM((48, D), BF16), pltpu.Sem...  1.75 us
    pallas_call x1, Pallas kernels, on_device(): call(project, 'project', 13, [shape((4, X_ROWS, LANES)), shape((16, LANES...  1.66 us

profile of v6, /device:TPU:2, one launch (start us, length us, event | category | flops | bytes accessed | tf_op | source)
XLA Modules:
  0.0 82.0 jit_solution(18028012850380263018)
XLA Ops:
  0.0 1.1 %partial_modulation.1 = bf16[8,24,128]{2,1,0:T(8,128)(2,1)S(1)} custom-call(bf16[1,64]{1,0:T(2,128)(2,1)} %cond_in.1, bf16[1,64]{1,0:T(2,128)(2,1)} %bitcast.12, bf16[64,1536]{1,0:T(8,128)(2,1)} %w_mod_in.1), custom_call_target="tpu_custom_call" | custom-call | flops 10000000000 | tf_op jit(solution)/shard_map/partial_modulation/pallas_call | solution.py:521
  1.1 16.5 %all_to_all.25.parts = bf16[8,24,128]{2,1,0:T(8,128)(2,1)S(1)} all-to-all(bf16[8,24,128]{2,1,0:T(8,128)(2,1)S(1)} %partial_modulation.1), channel_id=1, replica_groups=mesh['z'=8,'x'=4,'tp'=4,'dp'=2] {'z'}, dimensions={0} | all-to-all | bytes 98304 | tf_op jit(solution)/shard_map/all_to_all | solution.py:514
  17.6 0.0 copy-start.5
  17.6 0.0 copy-start.6
  17.6 0.0 copy-start.7
  17.6 0.0 copy-start.8
  17.7 0.0 copy-start.9
  17.7 0.0 copy-start.10
  17.7 0.0 copy-start.11
  17.7 0.0 copy-start.12
  17.7 13.9 %all_to_all.26.parts = bf16[16,24,128]{2,1,0:T(8,128)(2,1)S(1)} all-to-all(bf16[16,24,128]{2,1,0:T(8,128)(2,1)S(1)} %sum_and_spread.1), channel_id=1, replica_groups=mesh['z'=8,'x'=4,'tp'=4,'dp'=2] {'x','tp'}, dimensions={0} | all-to-all | bytes 196608 | tf_op jit(solution)/shard_map/all_to_all | solution.py:514
  31.6 0.0 copy-done.1
  31.6 0.0 copy-done.2
  31.6 0.0 copy-done.3
  31.6 0.0 copy-done.4
  31.6 0.0 copy-done.5
  31.6 0.0 copy-done.6
  31.6 0.0 copy-done.7
  31.6 0.0 copy-done.8
  31.6 0.0 copy-done.9
  31.7 0.0 copy-done.10
  31.7 0.0 copy-done.11
  31.7 0.0 copy-done.12
  31.7 0.0 copy-start
  31.7 0.0 copy-start.13
  31.7 1.7 %project.1 = (bf16[4,624,128]{2,1,0:T(8,128)(2,1)S(1)}, f32[16,128]{1,0:T(8,128)S(1)}) custom-call(bf16[16,24,128]{2,1,0:T(8,128)(2,1)S(1)} %all_to_all.26.parts, bf16[16,128]{1,0:T(8,128)(2,1)S(1)} %bitcast.10, bf16[1,192,2048]{2,1,0:T(8,128)(2,1)S(1)} %copy-done.1, bf16[1,8,2048]{2,1,0:T(8,128)(2,1)S(1)} %copy-done.6, bf16[2048,256]{1,0:T(8,128)(2,1)S(1)} %copy-done.2, ...), custom_call_target="tpu_custom_call" | custom-call | tf_op jit(solution)/shard_map/project/pallas_call | solution.py:535
  33.4 11.2 %all_to_all.27.got.sent = bf16[4,624,128]{2,1,0:T(8,128)(2,1)S(1)} all-to-all(bf16[4,624,128]{2,1,0:T(8,128)(2,1)S(1)} %get-tuple-element.10), channel_id=1, replica_groups=mesh['z'=8,'x'=4,'tp'=4,'dp'=2] {'x'}, dimensions={0} | all-to-all | bytes 1277952 | tf_op jit(solution)/shard_map/all_to_all | solution.py:514
  44.5 5.1 %token_maps.1 = (bf16[8,128,256]{2,1,0:T(8,128)(2,1)S(1)}, bf16[768,256]{1,0:T(8,128)(2,1)S(1)}, f32[768,128]{1,0:T(8,128)S(1)}) custom-call(bf16[4,624,128]{2,1,0:T(8,128)(2,1)S(1)} %all_to_all.27.got.sent), custom_call_target="tpu_custom_call" | custom-call | tf_op jit(solution)/shard_map/token_maps/pallas_call | solution.py:543
  49.7 16.2 %all_to_all.28.got = bf16[8,128,256]{2,1,0:T(8,128)(2,1)S(1)} all-to-all(bf16[8,128,256]{2,1,0:T(8,128)(2,1)S(1)} %get-tuple-element.11), channel_id=1, replica_groups=mesh['z'=8,'x'=4,'tp'=4,'dp'=2] {'z'}, dimensions={0} | all-to-all | bytes 1048576 | tf_op jit(solution)/shard_map/all_to_all | solution.py:514
  65.8 3.2 %read_states.1 = bf16[16,48,128]{2,1,0:T(8,128)(2,1)S(1)} custom-call(bf16[8,128,256]{2,1,0:T(8,128)(2,1)S(1)} %all_to_all.28.got, bf16[768,256]{1,0:T(8,128)(2,1)S(1)} %get-tuple-element.12.reads, f32[768,128]{1,0:T(8,128)S(1)} %get-tuple-element.13.offsets, bf16[4,624,128]{2,1,0:T(8,128)(2,1)S(1)} %all_to_all.27.got.sent), custom_call_target="tpu_custom_call" | custom-call | tf_op jit(solution)/shard_map/read_states/pallas_call | solution.py:551
  69.1 11.2 %all_to_all.29.got = bf16[16,48,128]{2,1,0:T(8,128)(2,1)S(1)} all-to-all(bf16[16,48,128]{2,1,0:T(8,128)(2,1)S(1)} %read_states.1), channel_id=1, replica_groups=mesh['z'=8,'x'=4,'tp'=4,'dp'=2] {'x','tp'}, dimensions={0} | all-to-all | bytes 393216 | tf_op jit(solution)/shard_map/all_to_all | solution.py:514
  80.2 1.8 %mix.1 = bf16[48,2048]{1,0:T(8,128)(2,1)} custom-call(bf16[16,48,128]{2,1,0:T(8,128)(2,1)S(1)} %all_to_all.29.got, bf16[1,128]{1,0:T(2,128)(2,1)S(1)} %bitcast.11, f32[16,128]{1,0:T(8,128)S(1)} %get-tuple-element.14.gate, bf16[1024,2048]{1,0:T(8,128)(2,1)S(1)} %copy-done, bf16[192,2048]{1,0:T(8,128)(2,1)S(1)} %bitcast.7), custom_call_target="tpu_custom_call" | custom-call | tf_op jit(solution)/shard_map/mix/pallas_call | solution.py:555
  (7 shorter events, 0.0 us)
Async XLA Ops:
  17.6 14.0 %copy-start.1 = (bf16[1,192,2048]{2,1,0:T(8,128)(2,1)S(1)}, bf16[1,192,2048]{2,1,0:T(8,128)(2,1)}, u32[]{:S(2)}) copy-start(bf16[1,192,2048]{2,1,0:T(8,128)(2,1)} %latent.1) | copy-start | bytes 2359300
  17.6 14.0 %copy-start.2 = (bf16[2048,256]{1,0:T(8,128)(2,1)S(1)}, bf16[2048,256]{1,0:T(8,128)(2,1)}, u32[]{:S(2)}) copy-start(bf16[2048,256]{1,0:T(8,128)(2,1)} %w_key.1) | copy-start | bytes 3145732
  17.6 14.0 %copy-start.3 = (bf16[2048,256]{1,0:T(8,128)(2,1)S(1)}, bf16[2048,256]{1,0:T(8,128)(2,1)}, u32[]{:S(2)}) copy-start(bf16[2048,256]{1,0:T(8,128)(2,1)} %w_value.1) | copy-start | bytes 3145732
  17.6 14.0 %copy-start.4 = (bf16[2048,256]{1,0:T(8,128)(2,1)S(1)}, bf16[2048,256]{1,0:T(8,128)(2,1)}, u32[]{:S(2)}) copy-start(bf16[2048,256]{1,0:T(8,128)(2,1)} %w_query.1) | copy-start | bytes 3145732
  17.6 14.0 %copy-start.5 = (bf16[2048,256]{1,0:T(8,128)(2,1)S(1)}, bf16[2048,256]{1,0:T(8,128)(2,1)}, u32[]{:S(2)}) copy-start(bf16[2048,256]{1,0:T(8,128)(2,1)} %w_gate.1) | copy-start | bytes 3145732
  17.6 14.0 %copy-start.6 = (bf16[1,8,2048]{2,1,0:T(8,128)(2,1)S(1)}, bf16[1,8,2048]{2,1,0:T(8,128)(2,1)}, u32[]{:S(2)}) copy-start(bf16[1,8,2048]{2,1,0:T(8,128)(2,1)} %context.1) | copy-start | bytes 98308
  17.6 14.0 %copy-start.7 = (bf16[2048,2,2]{0,2,1:T(2,128)(2,1)S(1)}, bf16[2048,2,2]{0,2,1:T(2,128)(2,1)}, u32[]{:S(2)}) copy-start(bf16[2048,2,2]{0,2,1:T(2,128)(2,1)} %param.27) | copy-start | bytes 49156
  17.6 14.0 %copy-start.8 = (bf16[2048,2,2]{0,2,1:T(2,128)(2,1)S(1)}, bf16[2048,2,2]{0,2,1:T(2,128)(2,1)}, u32[]{:S(2)}) copy-start(bf16[2048,2,2]{0,2,1:T(2,128)(2,1)} %param.28) | copy-start | bytes 49156
  17.7 14.0 %copy-start.9 = (bf16[2048]{0:T(1024)(128)(2,1)S(1)}, bf16[2048]{0:T(1024)(128)(2,1)}, u32[]{:S(2)}) copy-start(bf16[2048]{0:T(1024)(128)(2,1)} %param.22) | copy-start | bytes 12292
  17.7 14.0 %copy-start.10 = (f32[1,2,2,192]{3,2,1,0:T(2,128)S(1)}, f32[1,2,2,192]{3,2,1,0:T(2,128)}, u32[]{:S(2)}) copy-start(f32[1,2,2,192]{3,2,1,0:T(2,128)} %extra.1) | copy-start | bytes 9220
  17.7 14.0 %copy-start.11 = (f32[2,2]{1,0:T(2,128)S(1)}, f32[2,2]{1,0:T(2,128)}, u32[]{:S(2)}) copy-start(f32[2,2]{1,0:T(2,128)} %rate_at.1) | copy-start | bytes 52
  17.7 14.0 %copy-start.12 = (f32[2,2]{1,0:T(2,128)S(1)}, f32[2,2]{1,0:T(2,128)}, u32[]{:S(2)}) copy-start(f32[2,2]{1,0:T(2,128)} %bias_at.1) | copy-start | bytes 52
  31.7 48.6 %copy-start = (bf16[1024,2048]{1,0:T(8,128)(2,1)S(1)}, bf16[1024,2048]{1,0:T(8,128)(2,1)}, u32[]{:S(2)}) copy-start(bf16[1024,2048]{1,0:T(8,128)(2,1)} %w_out.1) | copy-start | bytes 12582916
  31.7 48.5 %copy-start.13 = (bf16[128]{0:T(256)(128)(2,1)S(1)}, bf16[128]{0:T(256)(128)(2,1)}, u32[]{:S(2)}) copy-start(bf16[128]{0:T(256)(128)(2,1)} %param.32) | copy-start | bytes 772
